TPU v7x, 512 devices: a whole 4x8x8 slice. The times are simulated.
512 devices in a mesh: sp: 64 (over z, y), tp: 8 (over x, core).
Axes of the slice: x: 4, y: 8, z: 8, core: 2. Of those that a mesh axis runs over, the one named last changes fastest.
Arguments:
- tokens: bfloat16 [24576, 2048], P('sp', 'tp'), may hold values from -60 to 60
- pre_gain: bfloat16 [2048], P('tp'), may hold values from 0.099609375 to 1.8984375
- w_query: bfloat16 [2048, 1024], P('sp', 'tp'), may hold values from -1 to 1
- w_key: bfloat16 [2048, 1024], P('sp', 'tp'), may hold values from -1 to 1
- w_value: bfloat16 [2048, 1024], P('sp', 'tp'), may hold values from -0.125 to 0.125
- w_pool: bfloat16 [2048, 1024], P('sp', 'tp'), may hold values from -0.125 to 0.125
- lambdas: float32 [8], P('tp'), may hold values from 0.3 to 0.8
- sub_gain: float32 [128], replicated, may hold values from 0.1 to 1.9
- group_weight: bfloat16 [8, 128, 128], P('tp'), may hold values from -0.5 to 0.5
- pool_scale: float32 [1024], P('tp'), may hold values from 0.1 to 1.9
- w_out: bfloat16 [2048, 2048], P('tp', 'sp'), may hold values from -0.125 to 0.125
Outputs:
- mixed_out: bfloat16 [24576, 2048], P(('sp', 'tp'))
All inputs are finite; a program needn't handle non-finite values.
Results may differ from a plain program's by a relative error of at most 0.015.
Values may be sent and summed in bfloat16 or wider, within the bound.
A program may use at most 128 MiB of HBM per device.

v0:
```python
import math

import jax
import jax.numpy as jnp
from jax import lax
from jax.sharding import PartitionSpec as P

EPSILON = 1e-06
NEG_LARGE = -1e30
WINDOWS = (2, 4, 8, 16)
RIM_ROWS = 15


def rows_first(arrays, axis, dims):
    turned = [jnp.moveaxis(a, dim, 0) for a, dim in zip(arrays, dims)]
    widths = [t[0].size for t in turned]
    both = jnp.concatenate([t.reshape(-1, w) for t, w in zip(turned, widths)], axis=1)
    filled = lax.all_gather(both, axis, axis=0, tiled=True)
    parts = jnp.split(filled, [sum(widths[:k]) for k in range(1, len(widths))], axis=1)
    return tuple(
        (
            jnp.moveaxis(b.reshape(-1, *t.shape[1:]), 0, dim)
            for b, t, dim in zip(parts, turned, dims)
        )
    )


def in_one_piece(arrays, axis, dim, along):
    both = jnp.concatenate(arrays, axis=along)
    filled, at, finished = (lax.all_gather(both, axis, axis=dim, tiled=True), 0, [])
    for a in arrays:
        finished.append(lax.slice_in_dim(filled, at, at + a.shape[along], axis=along))
        at += a.shape[along]
    return tuple(finished)


def passed_along(block, axis, distance):
    devices = range(lax.axis_size(axis))
    route = [(i - distance, i) for i in devices if i - distance in devices]
    return lax.ppermute(block, axis, route)


def unchanged(carried):
    return carried


def local(
    tokens,
    pre_gain,
    w_query,
    w_key,
    w_value,
    w_pool,
    lambdas,
    sub_gain,
    group_weight,
    pool_scale,
    w_out,
):
    tok_rows = tokens.shape[0]
    model_width = tokens.shape[1] * lax.axis_size("tp")
    local_heads = lambdas.shape[0]
    head_dim = w_query.shape[1] // (2 * local_heads)
    value_dim = w_value.shape[1] // local_heads
    local_groups = group_weight.shape[0]
    group_dim = group_weight.shape[1]
    q_cols = w_query.shape[1]
    v_cols = w_value.shape[1]
    w_cat = jnp.concatenate([w_query, w_key, w_value, w_pool], axis=1)
    w_in_full, w_out_rows = rows_first((w_cat, w_out), "sp", (0, 1))
    gain_row = pre_gain.reshape(1, -1)
    pieces = in_one_piece((tokens, gain_row), "tp", 1, 0)
    feature_part = pieces[0].astype(jnp.float32)
    scaled = (feature_part * pieces[1].astype(jnp.float32)).astype(jnp.bfloat16)
    projection = jnp.dot(scaled, w_in_full, preferred_element_type=jnp.float32)
    projection, squares = (projection, jnp.sum(feature_part * feature_part, axis=1))
    inverse = lax.rsqrt(squares / model_width + EPSILON)
    projected = (projection * inverse[:, None]).astype(jnp.bfloat16)
    queries = projected[:, :q_cols].reshape(tok_rows, local_heads, 2, head_dim)
    key_rows = projected[:, q_cols : 2 * q_cols]
    values = projected[:, 2 * q_cols : 2 * q_cols + v_cols]
    pool_in = projected[:, 2 * q_cols + v_cols :]
    first_row = lax.axis_index("sp") * tok_rows
    positions = first_row + jnp.arange(tok_rows, dtype=jnp.int32)
    shard_group = tok_rows * max(1, 1024 // tok_rows)
    score_scale = 1.0 / math.sqrt(head_dim)
    last_query = first_row + tok_rows - 1
    initial_max = jnp.full((local_heads, 2, tok_rows), NEG_LARGE, jnp.float32)
    initial_sum = jnp.zeros((local_heads, 2, tok_rows), jnp.float32)
    initial_weighted = jnp.zeros((local_heads, 2, tok_rows, value_dim), jnp.float32)
    pieces = in_one_piece((key_rows, values), "sp", 0, 1)
    key_piece = pieces[0].reshape(-1, local_heads, 2, head_dim)
    value_piece = pieces[1].reshape(-1, local_heads, value_dim)
    length = key_piece.shape[0]
    block_len = math.gcd(length, shard_group)

    def one_block(block_index, state):
        block_start = block_index * block_len

        def compute(inner):
            running_max, running_sum, weighted = inner
            key_block = lax.dynamic_slice_in_dim(key_piece, block_start, block_len, 0)
            value_block = lax.dynamic_slice_in_dim(value_piece, block_start, block_len, 0)
            scores = (
                jnp.einsum(
                    "qhmd,khmd->hmqk", queries, key_block, preferred_element_type=jnp.float32
                )
                * score_scale
            )
            key_pos = block_start + jnp.arange(block_len, dtype=jnp.int32)
            allowed = key_pos[None, :] <= positions[:, None]
            scores = jnp.where(allowed, scores, NEG_LARGE)
            new_max = jnp.maximum(running_max, jnp.max(scores, axis=-1))
            factor = jnp.exp(running_max - new_max)
            expo = jnp.where(allowed, jnp.exp(scores - new_max[..., None]), 0.0)
            running_sum = running_sum * factor + jnp.sum(expo, axis=-1)
            weighted = weighted * factor[..., None] + jnp.einsum(
                "hmqk,khd->hmqd",
                expo.astype(jnp.bfloat16),
                value_block,
                preferred_element_type=jnp.float32,
            )
            return (new_max, running_sum, weighted)

        return lax.cond(block_start <= last_query, compute, unchanged, state)

    running_max, running_sum, weighted = lax.fori_loop(
        0, length // block_len, one_block, (initial_max, initial_sum, initial_weighted)
    )
    head_mix = (
        weighted[:, 0] / running_sum[:, 0, :, None]
        - lambdas[:, None, None] * weighted[:, 1] / running_sum[:, 1, :, None]
    )
    mean_sq = jnp.mean(head_mix * head_mix, axis=-1, keepdims=True)
    normed = head_mix * lax.rsqrt(mean_sq + EPSILON) * sub_gain
    attention = jnp.transpose(normed, (1, 0, 2)).astype(jnp.bfloat16)
    halo_rows = passed_along(pool_in[tok_rows - RIM_ROWS :], "sp", 1)
    extended = jnp.concatenate([halo_rows, pool_in], axis=0).astype(jnp.float32)
    running = jnp.concatenate(
        [jnp.zeros((1, extended.shape[1]), jnp.float32), jnp.cumsum(extended, axis=0)], axis=0
    )
    running_top = running[RIM_ROWS + 1 :]
    window_ids = (
        lax.axis_index("tp") * local_groups + jnp.arange(local_groups, dtype=jnp.int32)
    ) % len(WINDOWS)
    column_window = jnp.repeat(window_ids, group_dim)
    average = jnp.zeros_like(running_top)
    for window_slot, window_span in enumerate(WINDOWS):
        running_low = running[RIM_ROWS + 1 - window_span : RIM_ROWS + 1 - window_span + tok_rows]
        window_count = jnp.minimum(positions + 1, window_span).astype(jnp.float32)
        average = average + jnp.where(
            column_window[None, :] == window_slot,
            (running_top - running_low) / window_count[:, None],
            0.0,
        )
    differ = (
        (average - pool_in.astype(jnp.float32))
        .astype(jnp.bfloat16)
        .reshape(tok_rows, local_groups, group_dim)
    )
    pooled = jnp.einsum("tgc,gcd->tgd", differ, group_weight, preferred_element_type=jnp.float32)
    pooled = (pooled * pool_scale.reshape(local_groups, group_dim)).astype(jnp.bfloat16)
    branch = jnp.concatenate([attention, pooled], axis=2).reshape(tok_rows, -1)
    token_rows = lax.all_to_all(branch, "tp", split_axis=0, concat_axis=1, tiled=True)
    whole_out = lax.all_gather(w_out_rows, "tp", axis=0, tiled=True)
    result = jnp.dot(token_rows, whole_out, preferred_element_type=jnp.float32)
    return result.astype(jnp.bfloat16)


def solution(mesh):
    placed = (
        P("sp", "tp"),
        P("tp"),
        P("sp", "tp"),
        P("sp", "tp"),
        P("sp", "tp"),
        P("sp", "tp"),
        P("tp"),
        P(),
        P("tp", None, None),
        P("tp"),
        P("tp", "sp"),
    )
    return jax.shard_map(
        local, mesh=mesh, in_specs=placed, out_specs=P(("sp", "tp"), None), check_vma=False
    )
```

profile of v0, /device:TPU:496, one launch (start us, length us, event | category | flops | bytes accessed | tf_op | source)
XLA Modules:
  0.0 433.9 jit_solution(12058757009128040848)
XLA Ops:
  13.1 25.7 %all-gather.5.cloned.1.call-done = bf16[385,2048]{1,0:T(8,128)(2,1)} async-done(((bf16[385,256]{1,0:T(8,128)(2,1)}), bf16[385,2048]{1,0:T(8,128)(2,1)}) %all-gather.5.cloned.1.call-update) | async-done | bytes 1576976 | tf_op jit(solution)/shard_map/all_gather | solution.py:30
  41.4 82.4 %all-gather.7.cloned.1.call-done = bf16[2048,768]{1,0:T(8,128)(2,1)} async-done(((bf16[32,768]{1,0:T(8,128)(2,1)}), bf16[2048,768]{1,0:T(8,128)(2,1)}) %all-gather.7.cloned.1.call-update) | async-done | bytes 3145744 | tf_op jit(solution)/shard_map/all_gather | solution.py:18
  123.9 3.1 fusion.35
  127.7 2.3 slice_bitcast_fusion.1
  130.7 3.1 collective-permute-start
  133.9 2.3 collective-permute-done
  137.0 108.4 %all-gather.9.cloned.1.call-done = bf16[24576,256]{1,0:T(8,128)(2,1)} async-done(((bf16[384,256]{1,0:T(8,128)(2,1)}), bf16[24576,256]{1,0:T(8,128)(2,1)}) %all-gather.9.cloned.1.call-update) | async-done | bytes 12582928 | tf_op jit(solution)/shard_map/all_gather | solution.py:30
  245.4 10.1 %slice_bitcast_fusion = (bf16[24576,1,128]{2,0,1:T(8,128)(2,1)}, bf16[24576,128]{1,0:T(8,128)(2,1)}) fusion(bf16[24576,256]{1,0:T(8,128)(2,1)} %all-gather.9.cloned.1.call-done), kind=kLoop, calls=%fused_computation.30 | loop fusion | bytes 25165824 | tf_op jit(solution)/shard_map/reshape | solution.py:93
  255.6 8.6 %copy.39 = bf16[24576,128]{0,1:T(8,128)(2,1)} copy(bf16[24576,128]{1,0:T(8,128)(2,1)} %get-tuple-element.264) | data formatting | bytes 12582912 | tf_op jit(solution)/shard_map/slice | solution.py:32
  264.3 144.8 %while.18 = (s32[]{:T(128)}, f32[1,2,384]{2,1,0:T(2,128)S(1)}, f32[1,2,384]{2,1,0:T(2,128)S(1)}, f32[1,2,384,128]{3,2,1,0:T(8,128)S(1)}, s32[]{:T(128)}, /*index...) while((s32[]{:T(128)}, f32[1,2,384]{2,1,0:T(2,128)S(1)}, ...), condition=%wide.region_6.7_spmd.clone, body=%wide.region_1.6_spmd.clone.sunk | while | flops 234655104 | bytes 9597241 | solution.py:127
  264.3 4.5 %conditional.3 = ((f32[1,2,384]{2,1,0:T(2,128)S(1)}, f32[1,2,384]{2,1,0:T(2,128)S(1)}, f32[1,2,384,128]{3,2,1,0:T(8,128)S(1)})) conditional(s32[]{:T(128)} %convert_element_type.121, (f32[1,2,384]{2,1,0:T(2,128)S(1)}, f32[1,2,384]{2,1,0:T(2,128)S(1)}, f32[1,2,384,128]{3,2,1,0:T(8,128)S(1)}) %tuple.51, (s32[]{:T(128)}, s32[]{:T(128)}, ...), branch_computations={%region_2.0_spmd, %region_3.5_spmd} | conditional | flops 234655104 | bytes 9595474 | solution.py:125
  266.2 2.0 fusion.5
  268.9 4.5 %conditional.3 = ((f32[1,2,384]{2,1,0:T(2,128)S(1)}, f32[1,2,384]{2,1,0:T(2,128)S(1)}, f32[1,2,384,128]{3,2,1,0:T(8,128)S(1)})) conditional(s32[]{:T(128)} %convert_element_type.121, (f32[1,2,384]{2,1,0:T(2,128)S(1)}, f32[1,2,384]{2,1,0:T(2,128)S(1)}, f32[1,2,384,128]{3,2,1,0:T(8,128)S(1)}) %tuple.51, (s32[]{:T(128)}, s32[]{:T(128)}, ...), branch_computations={%region_2.0_spmd, %region_3.5_spmd} | conditional | flops 234655104 | bytes 9595474 | solution.py:125
  270.7 2.0 fusion.5
  273.4 4.5 %conditional.3 = ((f32[1,2,384]{2,1,0:T(2,128)S(1)}, f32[1,2,384]{2,1,0:T(2,128)S(1)}, f32[1,2,384,128]{3,2,1,0:T(8,128)S(1)})) conditional(s32[]{:T(128)} %convert_element_type.121, (f32[1,2,384]{2,1,0:T(2,128)S(1)}, f32[1,2,384]{2,1,0:T(2,128)S(1)}, f32[1,2,384,128]{3,2,1,0:T(8,128)S(1)}) %tuple.51, (s32[]{:T(128)}, s32[]{:T(128)}, ...), branch_computations={%region_2.0_spmd, %region_3.5_spmd} | conditional | flops 234655104 | bytes 9595474 | solution.py:125
  277.9 4.6 %conditional.3 = ((f32[1,2,384]{2,1,0:T(2,128)S(1)}, f32[1,2,384]{2,1,0:T(2,128)S(1)}, f32[1,2,384,128]{3,2,1,0:T(8,128)S(1)})) conditional(s32[]{:T(128)} %convert_element_type.121, (f32[1,2,384]{2,1,0:T(2,128)S(1)}, f32[1,2,384]{2,1,0:T(2,128)S(1)}, f32[1,2,384,128]{3,2,1,0:T(8,128)S(1)}) %tuple.51, (s32[]{:T(128)}, s32[]{:T(128)}, ...), branch_computations={%region_2.0_spmd, %region_3.5_spmd} | conditional | flops 234655104 | bytes 9595474 | solution.py:125
  279.8 2.0 fusion.5
  282.5 4.5 %conditional.3 = ((f32[1,2,384]{2,1,0:T(2,128)S(1)}, f32[1,2,384]{2,1,0:T(2,128)S(1)}, f32[1,2,384,128]{3,2,1,0:T(8,128)S(1)})) conditional(s32[]{:T(128)} %convert_element_type.121, (f32[1,2,384]{2,1,0:T(2,128)S(1)}, f32[1,2,384]{2,1,0:T(2,128)S(1)}, f32[1,2,384,128]{3,2,1,0:T(8,128)S(1)}) %tuple.51, (s32[]{:T(128)}, s32[]{:T(128)}, ...), branch_computations={%region_2.0_spmd, %region_3.5_spmd} | conditional | flops 234655104 | bytes 9595474 | solution.py:125
  284.4 2.0 fusion.5
  287.0 4.5 %conditional.3 = ((f32[1,2,384]{2,1,0:T(2,128)S(1)}, f32[1,2,384]{2,1,0:T(2,128)S(1)}, f32[1,2,384,128]{3,2,1,0:T(8,128)S(1)})) conditional(s32[]{:T(128)} %convert_element_type.121, (f32[1,2,384]{2,1,0:T(2,128)S(1)}, f32[1,2,384]{2,1,0:T(2,128)S(1)}, f32[1,2,384,128]{3,2,1,0:T(8,128)S(1)}) %tuple.51, (s32[]{:T(128)}, s32[]{:T(128)}, ...), branch_computations={%region_2.0_spmd, %region_3.5_spmd} | conditional | flops 234655104 | bytes 9595474 | solution.py:125
  291.5 4.5 %conditional.3 = ((f32[1,2,384]{2,1,0:T(2,128)S(1)}, f32[1,2,384]{2,1,0:T(2,128)S(1)}, f32[1,2,384,128]{3,2,1,0:T(8,128)S(1)})) conditional(s32[]{:T(128)} %convert_element_type.121, (f32[1,2,384]{2,1,0:T(2,128)S(1)}, f32[1,2,384]{2,1,0:T(2,128)S(1)}, f32[1,2,384,128]{3,2,1,0:T(8,128)S(1)}) %tuple.51, (s32[]{:T(128)}, s32[]{:T(128)}, ...), branch_computations={%region_2.0_spmd, %region_3.5_spmd} | conditional | flops 234655104 | bytes 9595474 | solution.py:125
  293.4 2.0 fusion.5
  296.1 4.5 %conditional.3 = ((f32[1,2,384]{2,1,0:T(2,128)S(1)}, f32[1,2,384]{2,1,0:T(2,128)S(1)}, f32[1,2,384,128]{3,2,1,0:T(8,128)S(1)})) conditional(s32[]{:T(128)} %convert_element_type.121, (f32[1,2,384]{2,1,0:T(2,128)S(1)}, f32[1,2,384]{2,1,0:T(2,128)S(1)}, f32[1,2,384,128]{3,2,1,0:T(8,128)S(1)}) %tuple.51, (s32[]{:T(128)}, s32[]{:T(128)}, ...), branch_computations={%region_2.0_spmd, %region_3.5_spmd} | conditional | flops 234655104 | bytes 9595474 | solution.py:125
  300.6 4.5 %conditional.3 = ((f32[1,2,384]{2,1,0:T(2,128)S(1)}, f32[1,2,384]{2,1,0:T(2,128)S(1)}, f32[1,2,384,128]{3,2,1,0:T(8,128)S(1)})) conditional(s32[]{:T(128)} %convert_element_type.121, (f32[1,2,384]{2,1,0:T(2,128)S(1)}, f32[1,2,384]{2,1,0:T(2,128)S(1)}, f32[1,2,384,128]{3,2,1,0:T(8,128)S(1)}) %tuple.51, (s32[]{:T(128)}, s32[]{:T(128)}, ...), branch_computations={%region_2.0_spmd, %region_3.5_spmd} | conditional | flops 234655104 | bytes 9595474 | solution.py:125
  302.5 2.0 fusion.5
  305.1 4.5 %conditional.3 = ((f32[1,2,384]{2,1,0:T(2,128)S(1)}, f32[1,2,384]{2,1,0:T(2,128)S(1)}, f32[1,2,384,128]{3,2,1,0:T(8,128)S(1)})) conditional(s32[]{:T(128)} %convert_element_type.121, (f32[1,2,384]{2,1,0:T(2,128)S(1)}, f32[1,2,384]{2,1,0:T(2,128)S(1)}, f32[1,2,384,128]{3,2,1,0:T(8,128)S(1)}) %tuple.51, (s32[]{:T(128)}, s32[]{:T(128)}, ...), branch_computations={%region_2.0_spmd, %region_3.5_spmd} | conditional | flops 234655104 | bytes 9595474 | solution.py:125
  307.0 2.0 fusion.5
  309.7 4.5 %conditional.3 = ((f32[1,2,384]{2,1,0:T(2,128)S(1)}, f32[1,2,384]{2,1,0:T(2,128)S(1)}, f32[1,2,384,128]{3,2,1,0:T(8,128)S(1)})) conditional(s32[]{:T(128)} %convert_element_type.121, (f32[1,2,384]{2,1,0:T(2,128)S(1)}, f32[1,2,384]{2,1,0:T(2,128)S(1)}, f32[1,2,384,128]{3,2,1,0:T(8,128)S(1)}) %tuple.51, (s32[]{:T(128)}, s32[]{:T(128)}, ...), branch_computations={%region_2.0_spmd, %region_3.5_spmd} | conditional | flops 234655104 | bytes 9595474 | solution.py:125
  314.2 4.5 %conditional.3 = ((f32[1,2,384]{2,1,0:T(2,128)S(1)}, f32[1,2,384]{2,1,0:T(2,128)S(1)}, f32[1,2,384,128]{3,2,1,0:T(8,128)S(1)})) conditional(s32[]{:T(128)} %convert_element_type.121, (f32[1,2,384]{2,1,0:T(2,128)S(1)}, f32[1,2,384]{2,1,0:T(2,128)S(1)}, f32[1,2,384,128]{3,2,1,0:T(8,128)S(1)}) %tuple.51, (s32[]{:T(128)}, s32[]{:T(128)}, ...), branch_computations={%region_2.0_spmd, %region_3.5_spmd} | conditional | flops 234655104 | bytes 9595474 | solution.py:125
  316.0 2.0 fusion.5
  318.7 4.5 %conditional.3 = ((f32[1,2,384]{2,1,0:T(2,128)S(1)}, f32[1,2,384]{2,1,0:T(2,128)S(1)}, f32[1,2,384,128]{3,2,1,0:T(8,128)S(1)})) conditional(s32[]{:T(128)} %convert_element_type.121, (f32[1,2,384]{2,1,0:T(2,128)S(1)}, f32[1,2,384]{2,1,0:T(2,128)S(1)}, f32[1,2,384,128]{3,2,1,0:T(8,128)S(1)}) %tuple.51, (s32[]{:T(128)}, s32[]{:T(128)}, ...), branch_computations={%region_2.0_spmd, %region_3.5_spmd} | conditional | flops 234655104 | bytes 9595474 | solution.py:125
  320.6 2.0 fusion.5
  323.2 4.5 %conditional.3 = ((f32[1,2,384]{2,1,0:T(2,128)S(1)}, f32[1,2,384]{2,1,0:T(2,128)S(1)}, f32[1,2,384,128]{3,2,1,0:T(8,128)S(1)})) conditional(s32[]{:T(128)} %convert_element_type.121, (f32[1,2,384]{2,1,0:T(2,128)S(1)}, f32[1,2,384]{2,1,0:T(2,128)S(1)}, f32[1,2,384,128]{3,2,1,0:T(8,128)S(1)}) %tuple.51, (s32[]{:T(128)}, s32[]{:T(128)}, ...), branch_computations={%region_2.0_spmd, %region_3.5_spmd} | conditional | flops 234655104 | bytes 9595474 | solution.py:125
  327.7 4.5 %conditional.3 = ((f32[1,2,384]{2,1,0:T(2,128)S(1)}, f32[1,2,384]{2,1,0:T(2,128)S(1)}, f32[1,2,384,128]{3,2,1,0:T(8,128)S(1)})) conditional(s32[]{:T(128)} %convert_element_type.121, (f32[1,2,384]{2,1,0:T(2,128)S(1)}, f32[1,2,384]{2,1,0:T(2,128)S(1)}, f32[1,2,384,128]{3,2,1,0:T(8,128)S(1)}) %tuple.51, (s32[]{:T(128)}, s32[]{:T(128)}, ...), branch_computations={%region_2.0_spmd, %region_3.5_spmd} | conditional | flops 234655104 | bytes 9595474 | solution.py:125
  329.6 2.0 fusion.5
  332.2 4.5 %conditional.3 = ((f32[1,2,384]{2,1,0:T(2,128)S(1)}, f32[1,2,384]{2,1,0:T(2,128)S(1)}, f32[1,2,384,128]{3,2,1,0:T(8,128)S(1)})) conditional(s32[]{:T(128)} %convert_element_type.121, (f32[1,2,384]{2,1,0:T(2,128)S(1)}, f32[1,2,384]{2,1,0:T(2,128)S(1)}, f32[1,2,384,128]{3,2,1,0:T(8,128)S(1)}) %tuple.51, (s32[]{:T(128)}, s32[]{:T(128)}, ...), branch_computations={%region_2.0_spmd, %region_3.5_spmd} | conditional | flops 234655104 | bytes 9595474 | solution.py:125
  334.1 2.0 fusion.5
  336.8 4.5 %conditional.3 = ((f32[1,2,384]{2,1,0:T(2,128)S(1)}, f32[1,2,384]{2,1,0:T(2,128)S(1)}, f32[1,2,384,128]{3,2,1,0:T(8,128)S(1)})) conditional(s32[]{:T(128)} %convert_element_type.121, (f32[1,2,384]{2,1,0:T(2,128)S(1)}, f32[1,2,384]{2,1,0:T(2,128)S(1)}, f32[1,2,384,128]{3,2,1,0:T(8,128)S(1)}) %tuple.51, (s32[]{:T(128)}, s32[]{:T(128)}, ...), branch_computations={%region_2.0_spmd, %region_3.5_spmd} | conditional | flops 234655104 | bytes 9595474 | solution.py:125
  341.3 4.5 %conditional.3 = ((f32[1,2,384]{2,1,0:T(2,128)S(1)}, f32[1,2,384]{2,1,0:T(2,128)S(1)}, f32[1,2,384,128]{3,2,1,0:T(8,128)S(1)})) conditional(s32[]{:T(128)} %convert_element_type.121, (f32[1,2,384]{2,1,0:T(2,128)S(1)}, f32[1,2,384]{2,1,0:T(2,128)S(1)}, f32[1,2,384,128]{3,2,1,0:T(8,128)S(1)}) %tuple.51, (s32[]{:T(128)}, s32[]{:T(128)}, ...), branch_computations={%region_2.0_spmd, %region_3.5_spmd} | conditional | flops 234655104 | bytes 9595474 | solution.py:125
  343.1 2.0 fusion.5
  345.8 4.5 %conditional.3 = ((f32[1,2,384]{2,1,0:T(2,128)S(1)}, f32[1,2,384]{2,1,0:T(2,128)S(1)}, f32[1,2,384,128]{3,2,1,0:T(8,128)S(1)})) conditional(s32[]{:T(128)} %convert_element_type.121, (f32[1,2,384]{2,1,0:T(2,128)S(1)}, f32[1,2,384]{2,1,0:T(2,128)S(1)}, f32[1,2,384,128]{3,2,1,0:T(8,128)S(1)}) %tuple.51, (s32[]{:T(128)}, s32[]{:T(128)}, ...), branch_computations={%region_2.0_spmd, %region_3.5_spmd} | conditional | flops 234655104 | bytes 9595474 | solution.py:125
  347.7 2.0 fusion.5
  350.3 4.5 %conditional.3 = ((f32[1,2,384]{2,1,0:T(2,128)S(1)}, f32[1,2,384]{2,1,0:T(2,128)S(1)}, f32[1,2,384,128]{3,2,1,0:T(8,128)S(1)})) conditional(s32[]{:T(128)} %convert_element_type.121, (f32[1,2,384]{2,1,0:T(2,128)S(1)}, f32[1,2,384]{2,1,0:T(2,128)S(1)}, f32[1,2,384,128]{3,2,1,0:T(8,128)S(1)}) %tuple.51, (s32[]{:T(128)}, s32[]{:T(128)}, ...), branch_computations={%region_2.0_spmd, %region_3.5_spmd} | conditional | flops 234655104 | bytes 9595474 | solution.py:125
  354.8 4.5 %conditional.3 = ((f32[1,2,384]{2,1,0:T(2,128)S(1)}, f32[1,2,384]{2,1,0:T(2,128)S(1)}, f32[1,2,384,128]{3,2,1,0:T(8,128)S(1)})) conditional(s32[]{:T(128)} %convert_element_type.121, (f32[1,2,384]{2,1,0:T(2,128)S(1)}, f32[1,2,384]{2,1,0:T(2,128)S(1)}, f32[1,2,384,128]{3,2,1,0:T(8,128)S(1)}) %tuple.51, (s32[]{:T(128)}, s32[]{:T(128)}, ...), branch_computations={%region_2.0_spmd, %region_3.5_spmd} | conditional | flops 234655104 | bytes 9595474 | solution.py:125
  356.7 2.0 fusion.5
  359.4 4.5 %conditional.3 = ((f32[1,2,384]{2,1,0:T(2,128)S(1)}, f32[1,2,384]{2,1,0:T(2,128)S(1)}, f32[1,2,384,128]{3,2,1,0:T(8,128)S(1)})) conditional(s32[]{:T(128)} %convert_element_type.121, (f32[1,2,384]{2,1,0:T(2,128)S(1)}, f32[1,2,384]{2,1,0:T(2,128)S(1)}, f32[1,2,384,128]{3,2,1,0:T(8,128)S(1)}) %tuple.51, (s32[]{:T(128)}, s32[]{:T(128)}, ...), branch_computations={%region_2.0_spmd, %region_3.5_spmd} | conditional | flops 234655104 | bytes 9595474 | solution.py:125
  361.2 2.0 fusion.5
  363.9 4.5 %conditional.3 = ((f32[1,2,384]{2,1,0:T(2,128)S(1)}, f32[1,2,384]{2,1,0:T(2,128)S(1)}, f32[1,2,384,128]{3,2,1,0:T(8,128)S(1)})) conditional(s32[]{:T(128)} %convert_element_type.121, (f32[1,2,384]{2,1,0:T(2,128)S(1)}, f32[1,2,384]{2,1,0:T(2,128)S(1)}, f32[1,2,384,128]{3,2,1,0:T(8,128)S(1)}) %tuple.51, (s32[]{:T(128)}, s32[]{:T(128)}, ...), branch_computations={%region_2.0_spmd, %region_3.5_spmd} | conditional | flops 234655104 | bytes 9595474 | solution.py:125
  368.4 4.5 %conditional.3 = ((f32[1,2,384]{2,1,0:T(2,128)S(1)}, f32[1,2,384]{2,1,0:T(2,128)S(1)}, f32[1,2,384,128]{3,2,1,0:T(8,128)S(1)})) conditional(s32[]{:T(128)} %convert_element_type.121, (f32[1,2,384]{2,1,0:T(2,128)S(1)}, f32[1,2,384]{2,1,0:T(2,128)S(1)}, f32[1,2,384,128]{3,2,1,0:T(8,128)S(1)}) %tuple.51, (s32[]{:T(128)}, s32[]{:T(128)}, ...), branch_computations={%region_2.0_spmd, %region_3.5_spmd} | conditional | flops 234655104 | bytes 9595474 | solution.py:125
  370.3 2.0 fusion.5
  372.9 4.5 %conditional.3 = ((f32[1,2,384]{2,1,0:T(2,128)S(1)}, f32[1,2,384]{2,1,0:T(2,128)S(1)}, f32[1,2,384,128]{3,2,1,0:T(8,128)S(1)})) conditional(s32[]{:T(128)} %convert_element_type.121, (f32[1,2,384]{2,1,0:T(2,128)S(1)}, f32[1,2,384]{2,1,0:T(2,128)S(1)}, f32[1,2,384,128]{3,2,1,0:T(8,128)S(1)}) %tuple.51, (s32[]{:T(128)}, s32[]{:T(128)}, ...), branch_computations={%region_2.0_spmd, %region_3.5_spmd} | conditional | flops 234655104 | bytes 9595474 | solution.py:125
  374.8 2.0 fusion.5
  377.4 4.5 %conditional.3 = ((f32[1,2,384]{2,1,0:T(2,128)S(1)}, f32[1,2,384]{2,1,0:T(2,128)S(1)}, f32[1,2,384,128]{3,2,1,0:T(8,128)S(1)})) conditional(s32[]{:T(128)} %convert_element_type.121, (f32[1,2,384]{2,1,0:T(2,128)S(1)}, f32[1,2,384]{2,1,0:T(2,128)S(1)}, f32[1,2,384,128]{3,2,1,0:T(8,128)S(1)}) %tuple.51, (s32[]{:T(128)}, s32[]{:T(128)}, ...), branch_computations={%region_2.0_spmd, %region_3.5_spmd} | conditional | flops 234655104 | bytes 9595474 | solution.py:125
  382.0 4.5 %conditional.3 = ((f32[1,2,384]{2,1,0:T(2,128)S(1)}, f32[1,2,384]{2,1,0:T(2,128)S(1)}, f32[1,2,384,128]{3,2,1,0:T(8,128)S(1)})) conditional(s32[]{:T(128)} %convert_element_type.121, (f32[1,2,384]{2,1,0:T(2,128)S(1)}, f32[1,2,384]{2,1,0:T(2,128)S(1)}, f32[1,2,384,128]{3,2,1,0:T(8,128)S(1)}) %tuple.51, (s32[]{:T(128)}, s32[]{:T(128)}, ...), branch_computations={%region_2.0_spmd, %region_3.5_spmd} | conditional | flops 234655104 | bytes 9595474 | solution.py:125
  383.8 2.0 fusion.5
  386.5 4.5 %conditional.3 = ((f32[1,2,384]{2,1,0:T(2,128)S(1)}, f32[1,2,384]{2,1,0:T(2,128)S(1)}, f32[1,2,384,128]{3,2,1,0:T(8,128)S(1)})) conditional(s32[]{:T(128)} %convert_element_type.121, (f32[1,2,384]{2,1,0:T(2,128)S(1)}, f32[1,2,384]{2,1,0:T(2,128)S(1)}, f32[1,2,384,128]{3,2,1,0:T(8,128)S(1)}) %tuple.51, (s32[]{:T(128)}, s32[]{:T(128)}, ...), branch_computations={%region_2.0_spmd, %region_3.5_spmd} | conditional | flops 234655104 | bytes 9595474 | solution.py:125
  388.3 2.0 fusion.5
  391.0 4.5 %conditional.3 = ((f32[1,2,384]{2,1,0:T(2,128)S(1)}, f32[1,2,384]{2,1,0:T(2,128)S(1)}, f32[1,2,384,128]{3,2,1,0:T(8,128)S(1)})) conditional(s32[]{:T(128)} %convert_element_type.121, (f32[1,2,384]{2,1,0:T(2,128)S(1)}, f32[1,2,384]{2,1,0:T(2,128)S(1)}, f32[1,2,384,128]{3,2,1,0:T(8,128)S(1)}) %tuple.51, (s32[]{:T(128)}, s32[]{:T(128)}, ...), branch_computations={%region_2.0_spmd, %region_3.5_spmd} | conditional | flops 234655104 | bytes 9595474 | solution.py:125
  395.5 4.5 %conditional.3 = ((f32[1,2,384]{2,1,0:T(2,128)S(1)}, f32[1,2,384]{2,1,0:T(2,128)S(1)}, f32[1,2,384,128]{3,2,1,0:T(8,128)S(1)})) conditional(s32[]{:T(128)} %convert_element_type.121, (f32[1,2,384]{2,1,0:T(2,128)S(1)}, f32[1,2,384]{2,1,0:T(2,128)S(1)}, f32[1,2,384,128]{3,2,1,0:T(8,128)S(1)}) %tuple.51, (s32[]{:T(128)}, s32[]{:T(128)}, ...), branch_computations={%region_2.0_spmd, %region_3.5_spmd} | conditional | flops 234655104 | bytes 9595474 | solution.py:125
  400.0 4.5 %conditional.3 = ((f32[1,2,384]{2,1,0:T(2,128)S(1)}, f32[1,2,384]{2,1,0:T(2,128)S(1)}, f32[1,2,384,128]{3,2,1,0:T(8,128)S(1)})) conditional(s32[]{:T(128)} %convert_element_type.121, (f32[1,2,384]{2,1,0:T(2,128)S(1)}, f32[1,2,384]{2,1,0:T(2,128)S(1)}, f32[1,2,384,128]{3,2,1,0:T(8,128)S(1)}) %tuple.51, (s32[]{:T(128)}, s32[]{:T(128)}, ...), branch_computations={%region_2.0_spmd, %region_3.5_spmd} | conditional | flops 234655104 | bytes 9595474 | solution.py:125
  401.9 2.0 fusion.5
  404.6 4.5 %conditional.3 = ((f32[1,2,384]{2,1,0:T(2,128)S(1)}, f32[1,2,384]{2,1,0:T(2,128)S(1)}, f32[1,2,384,128]{3,2,1,0:T(8,128)S(1)})) conditional(s32[]{:T(128)} %convert_element_type.121, (f32[1,2,384]{2,1,0:T(2,128)S(1)}, f32[1,2,384]{2,1,0:T(2,128)S(1)}, f32[1,2,384,128]{3,2,1,0:T(8,128)S(1)}) %tuple.51, (s32[]{:T(128)}, s32[]{:T(128)}, ...), branch_computations={%region_2.0_spmd, %region_3.5_spmd} | conditional | flops 234655104 | bytes 9595474 | solution.py:125
  409.9 10.8 %all_to_all.16 = bf16[8,48,256]{2,1,0:T(8,128)(2,1)S(1)} all-to-all(bf16[8,48,256]{2,1,0:T(8,128)(2,1)S(1)} %pad_maximum_fusion.1), channel_id=1, replica_groups=mesh['sp'=64,'tp'=8] {'tp'}, dimensions={0} | all-to-all | bytes 393216 | tf_op jit(solution)/shard_map/all_to_all | solution.py:164
  420.7 6.7 %convolution_convert_fusion = bf16[48,2048]{1,0:T(8,128)(2,1)} fusion(bf16[48,2048]{1,0:T(8,128)(2,1)S(1)} %bitcast.110, bf16[2048,2048]{0,1:T(8,128)(2,1)} %all-gather.11.cloned.1.call-done), kind=kOutput, calls=%fused_computation.35 | convolution fusion | flops 402751488 | bytes 8781824 | tf_op jit(solution)/shard_map/dot_general | solution.py:166
  (358 shorter events, 113.8 us)
Async XLA Ops:
  6.5 130.1 %copy-start = (bf16[1,128,128]{2,1,0:T(8,128)(2,1)S(1)}, bf16[1,128,128]{2,1,0:T(8,128)(2,1)}, u32[]{:S(2)}) copy-start(bf16[1,128,128]{2,1,0:T(8,128)(2,1)} %param.23) | copy-start | bytes 98308
  6.5 32.3 %all-gather.5.cloned.1.call-start = ((), (), s32[]{:S(2)}) async-start(), calls=%async_computation.1 | async-start | bytes 1806336 | tf_op jit(solution)/shard_map/all_gather | solution.py:30
  8.9 115.0 %all-gather.7.cloned.1.call-start = ((), (), s32[]{:S(2)}) async-start(), calls=%async_computation.2 | async-start | bytes 3194880 | tf_op jit(solution)/shard_map/all_gather | solution.py:18
  12.4 0.6 copy-start.1
  13.1 232.4 %all-gather.9.cloned.1.call-start = ((), (), s32[]{:S(2)}) async-start(), calls=%async_computation.3 | async-start | bytes 12779520 | tf_op jit(solution)/shard_map/all_gather | solution.py:30
  127.7 293.1 %all-gather.11.cloned.1.call-start = ((), (), s32[]{:S(2)}) async-start(), calls=%async_computation.4 | async-start | bytes 9437184 | tf_op jit(solution)/shard_map/all_gather | solution.py:165
  130.0 6.6 %copy-start.3 = (f32[128]{0:T(128)S(1)}, f32[128]{0:T(128)}, u32[]{:S(2)}) copy-start(f32[128]{0:T(128)} %param.24) | copy-start | bytes 1540
  130.7 5.5 %collective-permute-start = (bf16[15,128]{1,0:T(8,128)(2,1)S(1)}, bf16[15,128]{1,0:T(8,128)(2,1)S(1)}, u32[]{:S(2)}, u32[]{:S(2)}) collective-permute-start(bf16[15,128]{1,0:T(8,128)(2,1)S(1)} %slice.89), channel_id=1, source_target_pairs={{0,8},{8,16},{16,24},{24,32},{32,40},{40,48},{48,56},{56,64},{64,7... | collective-permute-start | bytes 11528 | tf_op jit(solution)/shard_map/ppermute | solution.py:40
  264.3 145.4 %copy-start.2 = (f32[128]{0:T(128)S(1)}, f32[128]{0:T(128)}, u32[]{:S(2)}) copy-start(f32[128]{0:T(128)} %param.22) | copy-start | bytes 1540
Sparse Core Ops, SparseCore 0:
  9.4 29.3 all-gather.4
  41.9 81.9 all-gather.6
  127.8 117.6 all-gather.8
  247.4 59.3 all-gather.10
where the time goes:
time: 436 us; the launch traced here: 434 us
  waiting for transfers between devices  219 us (50%)
  matrix products  123 us (28%)
  other arithmetic  33.4 us (8%)
  local copies, waits for them, and re-layouts  27.2 us (6%)
  between operations  14 us (3%)
  blocking collectives  10.8 us (2%)
    all_gather x2, waiting for transfers between devices, in_one_piece(): lax.all_gather(both, axis, axis=dim, tiled=True)  134 us
    all_gather x1, waiting for transfers between devices, rows_first(): filled = lax.all_gather(both, axis, axis=0, tiled=True)  82.4 us
    dot_general x32, matrix products, compute(): jnp.einsum('hmqk,khd->hmqd', expo.astype(jnp.bfloat16), value_block, pref...  62.6 us
    dot_general x32, matrix products, compute(): jnp.einsum('qhmd,khmd->hmqk', queries, key_block, preferred_element_type=...  50.1 us
    reduce_sum x32, other arithmetic, compute(): running_sum = running_sum * factor + jnp.sum(expo, axis=-1)  20.2 us
    all_to_all x1, blocking collectives, local(): lax.all_to_all(branch, 'tp', split_axis=0, concat_axis=1, tiled=True)  10.8 us
    reshape x1, local copies, waits for them, and re-layouts, local(): value_piece = pieces[1].reshape(-1, local_heads, value_dim)  10.1 us
  transfers between devices with their start and end apart: 5, of which 4 were waited for; matrix products, arithmetic and copies ran while one was open for 39% of the time, Pallas kernels for 0%

commit v1 on v0

v1 whole, which is shorter than its diff:
```python
import functools
import math

import jax
import jax.numpy as jnp
from jax import lax
from jax.experimental import pallas as pl
from jax.experimental.pallas import tpu as pltpu
from jax.sharding import PartitionSpec as P

MESH = pl.DeviceIdType.MESH
VMEM = pltpu.VMEM
EPSILON = 1e-06
NEG_LARGE = -1e30
F32, BF16 = jnp.float32, jnp.bfloat16
RIM = 16


def grid_of(sp):
    ny = 2 ** ((sp.bit_length() - 1) // 2)
    return sp // ny, ny


def vspec(n):
    return [pl.BlockSpec(memory_space=VMEM)] * n


def sds(*shape, dtype=BF16):
    return jax.ShapeDtypeStruct(shape, dtype)


def call(kernel, ins, outs, scratch=(), cid=None, limit=40 << 20, name=None, flops=1 << 24):
    params = dict(vmem_limit_bytes=limit)
    if cid is not None:
        params.update(collective_id=cid, has_side_effects=True)
    return pl.pallas_call(
        kernel,
        out_shape=tuple(outs),
        in_specs=vspec(len(ins)),
        out_specs=tuple(vspec(len(outs))),
        scratch_shapes=list(scratch),
        compiler_params=pltpu.CompilerParams(**params),
        cost_estimate=pl.CostEstimate(flops=flops, bytes_accessed=1 << 20, transcendentals=0),
        name=name,
    )(*ins)


def rcopy(src, dst, ssem, rsem, dev):
    return pltpu.make_async_remote_copy(
        src_ref=src, dst_ref=dst, send_sem=ssem, recv_sem=rsem, device_id=dev, device_id_type=MESH
    )


def greet(peers):
    barrier = pltpu.get_barrier_semaphore()
    for dev in peers:
        pl.semaphore_signal(barrier, inc=1, device_id=dev, device_id_type=MESH)
    pl.semaphore_wait(barrier, len(peers))


def hops(n, direction, sub):
    return n // 2 if (direction + sub) % 2 == 0 else (n - 1) // 2


class Ring:
    def __init__(self, n, me, dev, piece, subs, ssem, rsem):
        self.n, self.me, self.dev, self.piece, self.subs = n, me, dev, piece, subs
        self.ssem, self.rsem = ssem, rsem
        self.steps = n // 2

    def copy(self, d, sub, k):
        sign = 1 if d == 0 else -1
        block = (self.me - sign * k) % self.n
        ref = self.piece(block, sub)
        return rcopy(
            ref, ref, self.ssem.at[d, sub, k], self.rsem.at[d, sub, k], self.dev((self.me + sign) % self.n)
        )

    def step(self, k):
        for sub in range(self.subs):
            for d in range(2):
                if k > 0 and k - 1 < hops(self.n, d, sub):
                    self.copy(d, sub, k - 1).wait_recv()
                if k < hops(self.n, d, sub):
                    self.copy(d, sub, k).start()

    def finish(self):
        for k in range(self.steps):
            for sub in range(self.subs):
                for d in range(2):
                    if k < hops(self.n, d, sub):
                        self.copy(d, sub, k).wait_send()


def ring_sems(n, subs):
    return [pltpu.SemaphoreType.DMA((2, subs, n // 2)), pltpu.SemaphoreType.DMA((2, subs, n // 2))]


def gather_kernel(nz, ny, nx, tok_ref, w_ref, tok_full, w_full, ts, tr, ys, yr, zs, zr, as_, ar, bs, br):
    s, t = lax.axis_index("sp"), lax.axis_index("tp")
    z, y, x, c = s // ny, s % ny, t // 2, t % 2
    half = w_ref.shape[0] // 2
    partner = (s, x * 2 + 1 - c)
    across = [(s, ((x + d) % nx) * 2 + c) for d in range(1, nx)]
    along_y = [(z * ny + (y + d) % ny, t) for d in range(1, ny)]
    along_z = [(((z + d) % nz) * ny + y, t) for d in range(1, nz)]
    greet([partner] + across + along_y + along_z)

    ysends = [
        rcopy(w_ref.at[0:half], w_full.at[z, y, 0], ys.at[d], yr.at[d], along_y[d]) for d in range(ny - 1)
    ]
    zsends = [
        rcopy(w_ref.at[half:], w_full.at[z, y, 1], zs.at[d], zr.at[d], along_z[d]) for d in range(nz - 1)
    ]
    tsends = [rcopy(tok_ref, tok_full.at[t], ts.at[d], tr.at[d], across[d]) for d in range(nx - 1)]
    tsends.append(rcopy(tok_ref, tok_full.at[t], ts.at[nx - 1], tr.at[nx - 1], partner))
    for copy in ysends + zsends + tsends:
        copy.start()
    w_full[z, y, 0] = w_ref[0:half]
    w_full[z, y, 1] = w_ref[half:]
    tok_full[t] = tok_ref[...]

    def piece_a(block, sub):
        return w_full.at[block, sub * (ny // 2) : (sub + 1) * (ny // 2), 0]

    def piece_b(block, sub):
        return w_full.at[sub * (nz // 2) : (sub + 1) * (nz // 2), block, 1]

    ring_a = Ring(nz, z, lambda i: (i * ny + y, t), piece_a, 2, as_, ar)
    ring_b = Ring(ny, y, lambda i: (z * ny + i, t), piece_b, 2, bs, br)
    for copy in ysends:
        copy.wait_recv()
    ring_a.step(0)
    for copy in zsends:
        copy.wait_recv()
    ring_b.step(0)
    relays = []
    for k in range(1, max(ring_a.steps, ring_b.steps) + 1):
        if k <= ring_a.steps:
            ring_a.step(k)
        if k <= ring_b.steps:
            ring_b.step(k)
        if k == 1:
            for d in range(nx - 1):
                tsends[d].wait_recv()
                source = ((x - 1 - d) % nx) * 2 + c
                relays.append(
                    rcopy(tok_full.at[source], tok_full.at[source], ts.at[nx + d], tr.at[nx + d], partner)
                )
                relays[-1].start()
    tsends[-1].wait_recv()
    for copy in relays:
        copy.wait_recv()
    for copy in ysends + zsends + tsends + relays:
        copy.wait_send()
    ring_a.finish()
    ring_b.finish()


def project_kernel(tp, tok_ref, w_ref, qt_ref, k_ref, vt_ref, pool_ref, scaled, sq):
    rows, part = qt_ref.shape[1], tok_ref.shape[2]
    sq[...] = jnp.zeros_like(sq)
    for t in range(tp):
        x = tok_ref[t, 0:rows].astype(F32)
        gain = tok_ref[t, rows : rows + 1].astype(F32)
        squares = x * x
        for i in range(part // 128):
            sq[...] += squares[:, i * 128 : (i + 1) * 128]
        scaled[:, t * part : (t + 1) * part] = (x * gain).astype(BF16)
    inverse = lax.rsqrt(jnp.sum(sq[...], axis=1, keepdims=True) / (tp * part) + EPSILON)

    def project(at):
        out = jnp.dot(scaled[...], w_ref[:, at * 128 : at * 128 + 256], preferred_element_type=F32) * inverse
        return out[:, 0:128].astype(BF16), out[:, 128:256].astype(BF16)

    q, k = project(0)
    qt_ref[...] = jnp.transpose(q.astype(F32)).astype(BF16)
    k_ref[...] = k
    v, p = project(2)
    vt_ref[...] = jnp.transpose(v.astype(F32)).astype(BF16)
    pool_ref[...] = p


def spread_kernel(
    nz, ny, q_ref, k_ref, v_ref, p_ref, q_all, k_all, v_all, halo, zs, zr, ys, yr, hs, hr
):
    s, t = lax.axis_index("sp"), lax.axis_index("tp")
    z, y = s // ny, s % ny
    sp = nz * ny
    dev_z = lambda i: (i * ny + y, t)
    dev_y = lambda i: (z * ny + i, t)
    rows = p_ref.shape[0]
    nxt, prv = ((s + 1) % sp, t), ((s + sp - 1) % sp, t)
    peers = [dev_z((z + 1) % nz), dev_z((z + nz - 1) % nz), dev_y((y + 1) % ny), dev_y((y + ny - 1) % ny)]
    greet(peers + [nxt, prv])
    hcopy = rcopy(p_ref.at[rows - RIM :], halo, hs, hr, nxt)
    hcopy.start()
    q_all[y] = q_ref[...]
    k_all[z] = k_ref[...]
    v_all[z] = v_ref[...]
    qd = q_ref.shape[0] // 2
    ring_y = Ring(ny, y, dev_y, lambda b, i: q_all.at[b, i * qd : (i + 1) * qd], 2, ys, yr)
    ring_z = Ring(nz, z, dev_z, lambda b, i: (k_all if i == 0 else v_all).at[b], 2, zs, zr)
    for k in range(max(ring_y.steps, ring_z.steps) + 1):
        if k <= ring_z.steps:
            ring_z.step(k)
        if k <= ring_y.steps:
            ring_y.step(k)
    hcopy.wait_recv()
    hcopy.wait_send()
    ring_z.finish()
    ring_y.finish()


def attend_kernel(nz, ny, scale, q_all, k_all, v_all, acc_ref, st_ref):
    s = lax.axis_index("sp")
    z, y = s // ny, s % ny
    rows = q_all.shape[2]
    qd = q_all.shape[1] // 2
    vd = v_all.shape[1]
    lanes = 2 * rows
    width = min(256, rows)
    factor = scale / math.log(2.0)

    def chunk(yq, _):
        qt = q_all[yq]
        low = lax.broadcasted_iota(jnp.int32, qt.shape, 0) < qd
        zero = jnp.zeros_like(qt)
        qz = jnp.concatenate([jnp.where(low, qt, zero), jnp.where(low, zero, qt)], axis=1)
        st_ref[yq, 0:1] = jnp.full((1, lanes), NEG_LARGE, F32)
        st_ref[yq, 1:8] = jnp.zeros((7, lanes), F32)
        acc_ref[yq] = jnp.zeros((vd, lanes), F32)

        def pair(p, masked):
            keys = k_all[pl.ds(2 * p, 2)].reshape(2 * rows, 2 * qd)
            vals = jnp.concatenate([v_all[2 * p], v_all[2 * p + 1]], axis=1)
            for at in range(0, lanes, width):
                cols = slice(at, at + width)
                sc = jnp.dot(keys, qz[:, cols], preferred_element_type=F32)
                if masked:
                    lane = lax.broadcasted_iota(jnp.int32, (1, width), 1) + at
                    lane = jnp.where(lane >= rows, lane - rows, lane)
                    qpos = lane + (z * ny + yq) * rows
                    sub = lax.broadcasted_iota(jnp.int32, (2 * rows, 1), 0)
                    kpos = sub + (2 * p * ny + y) * rows
                    kpos = jnp.where(sub >= rows, kpos + (ny - 1) * rows, kpos)
                    allowed = kpos <= qpos
                    sc = jnp.where(allowed, sc, NEG_LARGE)
                old = st_ref[yq, 0:1, cols]
                new = jnp.maximum(old, jnp.max(sc, axis=0, keepdims=True))
                expo = jnp.exp2((sc - new) * factor)
                if masked:
                    expo = jnp.where(allowed, expo, 0.0)
                shrink = jnp.exp2((old - new) * factor)
                st_ref[yq, 0:1, cols] = new
                st_ref[yq, 1:2, cols] = st_ref[yq, 1:2, cols] * shrink + jnp.sum(expo, axis=0, keepdims=True)
                acc_ref[yq, :, cols] = acc_ref[yq, :, cols] * shrink + jnp.dot(
                    vals, expo.astype(BF16), preferred_element_type=F32
                )

        def full(p, carry):
            pair(p, False)
            return carry

        lax.fori_loop(0, z // 2, full, 0)

        @pl.when(jnp.logical_or(z % 2 == 1, yq >= y))
        def _():
            pair(z // 2, True)

        return 0

    lax.fori_loop(0, ny, chunk, 0)


def merge_kernel(ny, scale, acc_ref, st_ref, lam_ref, gain_ref, att_ref, mix, wbuf, sbuf, wland, sland, ws, wr, ss, sr):
    s, t = lax.axis_index("sp"), lax.axis_index("tp")
    z, y = s // ny, s % ny
    rows = att_ref.shape[0]
    factor = scale / math.log(2.0)
    dev = lambda i: (z * ny + i % ny, t)
    greet([dev(y + 1), dev(y + ny - 1)])

    def own(block, m):
        cols = slice(m * rows, (m + 1) * rows)
        return acc_ref[block, :, cols], st_ref[block, 0:1, cols], st_ref[block, 1:2, cols]

    def joined(a, b):
        top = jnp.maximum(a[1], b[1])
        fa, fb = jnp.exp2((a[1] - top) * factor), jnp.exp2((b[1] - top) * factor)
        return a[0] * fa + b[0] * fb, top, a[2] * fa + b[2] * fb

    def landed(d, m, k):
        return wland[d, m, k].astype(F32), sland[d, m, k, 0:1], sland[d, m, k, 1:2]

    def copies(d, m, k):
        to = dev(y + (1 if d == 0 else ny - 1))
        return [
            rcopy(wbuf.at[d, m, k], wland.at[d, m, k], ws.at[d, m, k], wr.at[d, m, k], to),
            rcopy(sbuf.at[d, m, k], sland.at[d, m, k], ss.at[d, m, k], sr.at[d, m, k], to),
        ]

    for k in range(ny // 2):
        for m in range(2):
            for d in range(2):
                n = hops(ny, d, m)
                if k >= n:
                    continue
                sign = 1 if d == 0 else -1
                block = (y + sign * (n - k)) % ny
                state = own(block, m)
                if k > 0:
                    for copy in copies(d, m, k - 1):
                        copy.wait_recv()
                    state = joined(state, landed(d, m, k - 1))
                wbuf[d, m, k] = state[0].astype(BF16)
                sbuf[d, m, k, 0:1] = state[1]
                sbuf[d, m, k, 1:2] = state[2]
                for copy in copies(d, m, k):
                    copy.start()
    for m in range(2):
        state = own(y, m)
        for d in range(2):
            n = hops(ny, d, m)
            if n > 0:
                for copy in copies(d, m, n - 1):
                    copy.wait_recv()
                state = joined(state, landed(d, m, n - 1))
        if m == 0:
            mix[...] = state[0] / state[2]
        else:
            mix[...] = mix[...] - lam_ref[0:1, 0:1] * state[0] / state[2]
    head = mix[...]
    mean = jnp.mean(head * head, axis=0, keepdims=True)
    normed = jnp.transpose(head * lax.rsqrt(mean + EPSILON)) * gain_ref[...]
    att_ref[...] = normed.astype(BF16)
    for k in range(ny // 2):
        for m in range(2):
            for d in range(2):
                if k < hops(ny, d, m):
                    for copy in copies(d, m, k):
                        copy.wait_send()


def output_kernel(p_ref, halo, gw_ref, ps_ref, att_ref, wo_ref, out_ref):
    s, t = lax.axis_index("sp"), lax.axis_index("tp")
    rows, dim = p_ref.shape
    here = p_ref[...].astype(F32)
    rim = jnp.where(s > 0, halo[...].astype(F32), 0.0)
    ext = jnp.concatenate([rim, here], axis=0)
    total = ext
    slot = t % 4
    for i in range(4):
        more = total + pltpu.roll(total, 1 << i, 0)
        total = jnp.where(i <= slot, more, total)
    span = jnp.where(slot == 0, 2, jnp.where(slot == 1, 4, jnp.where(slot == 2, 8, 16)))
    pos = s * rows + lax.broadcasted_iota(jnp.int32, (rows, 1), 0)
    count = jnp.minimum(pos + 1, span).astype(F32)
    differ = (total[RIM:] / count - here).astype(BF16)
    pooled = jnp.dot(differ, gw_ref[0], preferred_element_type=F32) * ps_ref[...]
    branch = jnp.concatenate([att_ref[...], pooled.astype(BF16)], axis=1)
    cols = wo_ref.shape[0]
    step = min(cols, 512)
    for at in range(0, cols, step):
        out_ref[:, at : at + step] = lax.dot_general(
            branch, wo_ref[at : at + step], (((1,), (1,)), ((), ())), preferred_element_type=F32
        ).astype(BF16)


def scatter_kernel(tp, part_ref, out_ref, land, ss, rs):
    s, t = lax.axis_index("sp"), lax.axis_index("tp")
    rows = out_ref.shape[0]
    peers = [(s, (t + d) % tp) for d in range(1, tp)]
    greet(peers)
    copies = []
    for d in range(1, tp):
        start = pl.multiple_of(((t + d) % tp) * rows, 16)
        copies.append(rcopy(part_ref.at[pl.ds(start, rows)], land.at[d - 1], ss.at[d - 1], rs.at[d - 1], peers[d - 1]))
        copies[-1].start()
    total = part_ref[pl.ds(pl.multiple_of(t * rows, 16), rows)].astype(F32)
    for d in range(1, tp):
        copies[d - 1].wait_recv()
        total = total + land[d - 1].astype(F32)
    out_ref[...] = total.astype(BF16)
    for copy in copies:
        copy.wait_send()


def local(sp, tp, tokens, pre_gain, w_query, w_key, w_value, w_pool, lambdas, sub_gain, group_weight, pool_scale, w_out):
    nz, ny = grid_of(sp)
    nx = tp // 2
    rows, part = tokens.shape
    wrows = w_query.shape[0]
    head = w_value.shape[1]
    qd = w_query.shape[1]
    wide = 2 * qd + 2 * head
    cols = w_out.shape[1]
    scale = 1.0 / math.sqrt(qd // 2)
    dma = pltpu.SemaphoreType.DMA
    tok = jnp.concatenate([tokens, jnp.broadcast_to(pre_gain[None], (16, part))], axis=0)
    wcat = jnp.concatenate([w_query, w_key, w_value, w_pool, w_out.T], axis=1)
    tok_full, w_full = call(
        functools.partial(gather_kernel, nz, ny, nx),
        (tok, wcat),
        (sds(tp, rows + 16, part), sds(nz, ny, 2, wrows // 2, wcat.shape[1])),
        [dma((2 * nx,)), dma((2 * nx,)), dma((ny,)), dma((ny,)), dma((nz,)), dma((nz,))]
        + ring_sems(nz, 2)
        + ring_sems(ny, 2),
        cid=0,
        name="gather",
    )
    w_all = w_full.reshape(sp * wrows, wcat.shape[1])
    qt, k, vt, pool = call(
        functools.partial(project_kernel, tp),
        (tok_full, w_all),
        (sds(qd, rows), sds(rows, qd), sds(head, rows), sds(rows, head)),
        [pltpu.VMEM((rows, tp * part), BF16), pltpu.VMEM((rows, 128), F32)],
        name="project",
    )
    q_all, k_all, v_all, halo = call(
        functools.partial(spread_kernel, nz, ny),
        (qt, k, vt, pool),
        (sds(ny, qd, rows), sds(nz, rows, qd), sds(nz, head, rows), sds(RIM, head)),
        ring_sems(nz, 2) + ring_sems(ny, 2) + [dma, dma],
        cid=1,
        name="spread",
    )
    acc, st = call(
        functools.partial(attend_kernel, nz, ny, scale),
        (q_all, k_all, v_all),
        (sds(ny, head, 2 * rows, dtype=F32), sds(ny, 8, 2 * rows, dtype=F32)),
        name="attend",
    )
    half = ny // 2
    (att,) = call(
        functools.partial(merge_kernel, ny, scale),
        (acc, st, jnp.broadcast_to(lambdas.reshape(1, 1), (8, 128)), sub_gain.reshape(1, head)),
        (sds(rows, head),),
        [
            pltpu.VMEM((head, rows), F32),
            pltpu.VMEM((2, 2, half, head, rows), BF16),
            pltpu.VMEM((2, 2, half, 8, rows), F32),
            pltpu.VMEM((2, 2, half, head, rows), BF16),
            pltpu.VMEM((2, 2, half, 8, rows), F32),
        ]
        + [dma((2, 2, half))] * 4,
        cid=2,
        name="merge",
    )
    (partial,) = call(
        output_kernel,
        (pool, halo, group_weight, pool_scale.reshape(1, head), att, w_all[:, wide:]),
        (sds(rows, sp * cols),),
        name="output",
    )
    out_rows = rows // tp
    (out,) = call(
        functools.partial(scatter_kernel, tp),
        (partial,),
        (sds(out_rows, sp * cols),),
        [pltpu.VMEM((tp - 1, out_rows, sp * cols), BF16), dma((tp - 1,)), dma((tp - 1,))],
        cid=3,
        name="scatter",
    )
    return out


def solution(mesh):
    placed = (
        P("sp", "tp"),
        P("tp"),
        P("sp", "tp"),
        P("sp", "tp"),
        P("sp", "tp"),
        P("sp", "tp"),
        P("tp"),
        P(),
        P("tp", None, None),
        P("tp"),
        P("tp", "sp"),
    )
    body = functools.partial(local, mesh.shape["sp"], mesh.shape["tp"])
    return jax.shard_map(body, mesh=mesh, in_specs=placed, out_specs=P(("sp", "tp"), None), check_vma=False)
```

time: 436 us -> 169 us (0.39)
  the two profiles are of different devices: /device:TPU:496 before, /device:TPU:449 now
where the time goes in v1:
time: 169 us; the launch traced here: 168 us
  Pallas kernels  162 us (96%)
  local copies, waits for them, and re-layouts  4.96 us (3%)
    pallas_call x7, Pallas kernels, call(): pl.pallas_call(kernel, out_shape=tuple(outs), in_specs=vspec(len(ins)), o...  162 us
    unnamed x11, local copies, waits for them, and re-layouts  3.51 us

profile of v1, /device:TPU:449, one launch (start us, length us, event | category | flops | bytes accessed | tf_op | source)
XLA Modules:
  0.0 168.4 jit_solution(12342694374100208472)
XLA Ops:
  0.7 0.7 broadcast_in_dim.6
  1.3 0.7 constant_dynamic-update-slice_fusion.3
  2.0 0.7 constant_dynamic-update-slice_fusion.2
  2.7 0.7 constant_dynamic-update-slice_fusion.1
  3.4 0.7 constant_dynamic-update-slice_fusion
  4.1 0.7 bitcast_dynamic-update-slice_fusion.w_ref
  4.9 0.9 pad_maximum_fusion.tok_ref
  5.8 32.2 %gather.1 = (bf16[8,400,256]{2,1,0:T(8,128)(2,1)S(1)}, bf16[8,8,2,16,768]{4,3,2,1,0:T(8,128)(2,1)S(1)}) custom-call(bf16[400,256]{1,0:T(8,128)(2,1)S(1)} %pad_maximum_fusion.tok_ref, bf16[32,768]{1,0:T(8,128)(2,1)S(1)} %bitcast_dynamic-update-slice_fusion.w_ref), custom_call_target="tpu_custom_call" | custom-call | flops 16777216 | bytes 1048576 | tf_op jit(solution)/shard_map/gather/pallas_call | solution.py:36
  38.0 1.1 project.1
  39.1 0.0 copy-start.1
  39.1 0.1 slice.4.wo_ref
  39.2 0.0 copy-start
  39.2 0.0 copy-start.2
  39.2 20.3 %spread.1 = (bf16[8,128,384]{2,1,0:T(8,128)(2,1)S(1)}, bf16[8,384,128]{2,1,0:T(8,128)(2,1)S(1)}, bf16[8,128,384]{2,1,0:T(8,128)(2,1)S(1)}, bf16[16,128]{1,0:T(8,128)(2,1)S(1)}) custom-call(bf16[128,384]{1,0:T(8,128)(2,1)S(1)} %get-tuple-element.20.q_ref, bf16[384,128]{1,0:T(8,128)(2,1)S(1)} %get-tuple-element.21.k_ref, ...), custom_call_target="tpu_custom_call" | custom-call | flops 16777216 | bytes 1048576 | tf_op jit(solution)/shard_map/spread/pallas_call | solution.py:36
  59.5 55.5 %attend.1 = (f32[8,128,768]{2,1,0:T(8,128)S(1)}, f32[8,8,768]{2,1,0:T(8,128)S(1)}) custom-call(bf16[8,128,384]{2,1,0:T(8,128)(2,1)S(1)} %get-tuple-element.24.q_all, bf16[8,384,128]{2,1,0:T(8,128)(2,1)S(1)} %get-tuple-element.25.k_all, bf16[8,128,384]{2,1,0:T(8,128)(2,1)S(1)} %get-tuple-element.26.v_all), custom_call_target="tpu_custom_call" | custom-call | flops 16777216 | bytes 1048576 | tf_op jit(solution)/shard_map/attend/pallas_call | solution.py:36
  115.0 0.0 copy-done.1
  115.0 20.1 %merge.1.att_ref = bf16[384,128]{1,0:T(8,128)(2,1)S(1)} custom-call(f32[8,128,768]{2,1,0:T(8,128)S(1)} %get-tuple-element.27.acc_ref, f32[8,8,768]{2,1,0:T(8,128)S(1)} %get-tuple-element.28.st_ref, f32[8,128]{1,0:T(8,128)S(1)} %broadcast_in_dim.15.lam_ref, f32[1,128]{1,0:T(1,128)S(1)} %bitcast.9), custom_call_target="tpu_custom_call" | custom-call | flops 16777216 | bytes 1048576 | tf_op jit(solution)/shard_map/merge/pallas_call | solution.py:36
  135.1 0.0 copy-done
  135.2 0.0 copy-done.2
  135.2 0.7 output.1.part_ref
  135.9 31.8 %scatter.1 = bf16[48,2048]{1,0:T(8,128)(2,1)S(1)} custom-call(bf16[384,2048]{1,0:T(8,128)(2,1)S(1)} %output.1.part_ref), custom_call_target="tpu_custom_call" | custom-call | flops 16777216 | bytes 1048576 | tf_op jit(solution)/shard_map/scatter/pallas_call | solution.py:36
  167.7 0.7 copy.18
  (1 shorter events, 0.0 us)
Async XLA Ops:
  39.1 75.9 %copy-start.1 = (f32[128]{0:T(128)S(1)}, f32[128]{0:T(128)}, u32[]{:S(2)}) copy-start(f32[128]{0:T(128)} %param.18) | copy-start | bytes 1540
  39.2 96.0 %copy-start = (bf16[1,128,128]{2,1,0:T(8,128)(2,1)S(1)}, bf16[1,128,128]{2,1,0:T(8,128)(2,1)}, u32[]{:S(2)}) copy-start(bf16[1,128,128]{2,1,0:T(8,128)(2,1)} %gw_ref.1) | copy-start | bytes 98308
  39.2 96.0 %copy-start.2 = (f32[128]{0:T(128)S(1)}, f32[128]{0:T(128)}, u32[]{:S(2)}) copy-start(f32[128]{0:T(128)} %param.20) | copy-start | bytes 1540

commit v2 on v1

--- a/solution.py
+++ b/solution.py
@@ -14,6 +14,8 @@
 NEG_LARGE = -1e30
 F32, BF16 = jnp.float32, jnp.bfloat16
 RIM = 16
+DEPTH = 256
+LEAD = 3
 
 
 def grid_of(sp):
@@ -96,10 +98,17 @@
     return [pltpu.SemaphoreType.DMA((2, subs, n // 2)), pltpu.SemaphoreType.DMA((2, subs, n // 2))]
 
 
-def gather_kernel(nz, ny, nx, tok_ref, w_ref, tok_full, w_full, ts, tr, ys, yr, zs, zr, as_, ar, bs, br):
+def gather_kernel(nz, ny, nx, tin_ref, gain_ref, wq_ref, wk_ref, wv_ref, wp_ref, tok_full, w_full, tok_ref, w_ref, ts, tr, ys, yr, zs, zr, as_, ar, bs, br):
     s, t = lax.axis_index("sp"), lax.axis_index("tp")
     z, y, x, c = s // ny, s % ny, t // 2, t % 2
     half = w_ref.shape[0] // 2
+    rows = tin_ref.shape[0]
+    tok_ref[0:rows] = tin_ref[...]
+    tok_ref[rows:] = jnp.broadcast_to(gain_ref[...], (16, gain_ref.shape[1]))
+    at = 0
+    for ref in (wq_ref, wk_ref, wv_ref, wp_ref):
+        w_ref[:, at : at + ref.shape[1]] = ref[...]
+        at += ref.shape[1]
     partner = (s, x * 2 + 1 - c)
     across = [(s, ((x + d) % nx) * 2 + c) for d in range(1, nx)]
     along_y = [(z * ny + (y + d) % ny, t) for d in range(1, ny)]
@@ -182,7 +191,7 @@
 
 
 def spread_kernel(
-    nz, ny, q_ref, k_ref, v_ref, p_ref, q_all, k_all, v_all, halo, zs, zr, ys, yr, hs, hr
+    nz, ny, q_ref, k_ref, v_ref, p_ref, wo_ref, q_all, k_all, v_all, halo, wo_all, zs, zr, ys, yr, os, or_, ws, wr, hs, hr
 ):
     s, t = lax.axis_index("sp"), lax.axis_index("tp")
     z, y = s // ny, s % ny
@@ -191,28 +200,44 @@
     dev_y = lambda i: (z * ny + i, t)
     rows = p_ref.shape[0]
     nxt, prv = ((s + 1) % sp, t), ((s + sp - 1) % sp, t)
-    peers = [dev_z((z + 1) % nz), dev_z((z + nz - 1) % nz), dev_y((y + 1) % ny), dev_y((y + ny - 1) % ny)]
-    greet(peers + [nxt, prv])
-    hcopy = rcopy(p_ref.at[rows - RIM :], halo, hs, hr, nxt)
-    hcopy.start()
+    along_z = [dev_z((z + d) % nz) for d in range(1, nz)]
+    greet(along_z + [dev_y((y + 1) % ny), dev_y((y + ny - 1) % ny), nxt, prv])
     q_all[y] = q_ref[...]
     k_all[z] = k_ref[...]
     v_all[z] = v_ref[...]
     qd = q_ref.shape[0] // 2
     ring_y = Ring(ny, y, dev_y, lambda b, i: q_all.at[b, i * qd : (i + 1) * qd], 2, ys, yr)
     ring_z = Ring(nz, z, dev_z, lambda b, i: (k_all if i == 0 else v_all).at[b], 2, zs, zr)
-    for k in range(max(ring_y.steps, ring_z.steps) + 1):
+    ring_z.step(0)
+    ring_y.step(0)
+    wcopies = [rcopy(wo_ref, wo_all.at[z, y], ws.at[d], wr.at[d], along_z[d]) for d in range(nz - 1)]
+    hcopy = rcopy(p_ref.at[rows - RIM :], halo, hs, hr, nxt)
+    for copy in wcopies + [hcopy]:
+        copy.start()
+    wo_all[z, y] = wo_ref[...]
+    ring_o = Ring(ny, y, dev_y, lambda b, i: wo_all.at[i * (nz // 2) : (i + 1) * (nz // 2), b], 2, os, or_)
+    for k in range(1, max(ring_y.steps, ring_z.steps) + 1):
         if k <= ring_z.steps:
             ring_z.step(k)
         if k <= ring_y.steps:
             ring_y.step(k)
+        if k == 1:
+            for copy in wcopies:
+                copy.wait_recv()
+            ring_o.step(0)
+        elif k - 1 <= ring_o.steps:
+            ring_o.step(k - 1)
+    for k in range(max(ring_y.steps, ring_z.steps), ring_o.steps + 1):
+        ring_o.step(k)
     hcopy.wait_recv()
-    hcopy.wait_send()
+    for copy in wcopies + [hcopy]:
+        copy.wait_send()
     ring_z.finish()
     ring_y.finish()
-
-
-def attend_kernel(nz, ny, scale, q_all, k_all, v_all, acc_ref, st_ref):
+    ring_o.finish()
+
+
+def attend_kernel(nz, ny, scale, q_all, k_all, v_all, acc_ref, st_ref, qz_ref, bar_ref, sum_ref):
     s = lax.axis_index("sp")
     z, y = s // ny, s % ny
     rows = q_all.shape[2]
@@ -222,64 +247,155 @@
     width = min(256, rows)
     factor = scale / math.log(2.0)
 
-    def chunk(yq, _):
+    def positions(yq, at, wide):
+        lane = lax.broadcasted_iota(jnp.int32, (1, wide), 1) + at
+        return jnp.where(lane >= rows, lane - rows, lane) + (z * ny + yq) * rows
+
+    def set_queries(yq):
         qt = q_all[yq]
         low = lax.broadcasted_iota(jnp.int32, qt.shape, 0) < qd
         zero = jnp.zeros_like(qt)
-        qz = jnp.concatenate([jnp.where(low, qt, zero), jnp.where(low, zero, qt)], axis=1)
+        qz_ref[:, 0:rows] = jnp.where(low, qt, zero)
+        qz_ref[:, rows:] = jnp.where(low, zero, qt)
+        acc_ref[yq] = jnp.zeros((vd, lanes), F32)
+
+    def tiles(yq, keys, vals, mask):
+        depth = keys.shape[0] if keys.shape[0] == rows else min(DEPTH, rows)
+        work = [(at, low) for at in range(0, lanes, width) for low in range(0, keys.shape[0], depth)]
+
+        def scores(item):
+            at, low = item
+            return jnp.dot(keys[low : low + depth], qz_ref[:, at : at + width], preferred_element_type=F32)
+
+        ahead = [scores(item) for item in work[:LEAD]]
+        total, gain = None, None
+        for i, (at, low) in enumerate(work):
+            sc = ahead.pop(0)
+            if i + LEAD < len(work):
+                ahead.append(scores(work[i + LEAD]))
+            cols = slice(at, at + width)
+            expo = jnp.exp2(sc * factor - bar_ref[0:1, cols])
+            if mask is not None:
+                expo = jnp.where(mask(at)[low : low + depth], expo, 0.0)
+            part = jnp.sum(expo.reshape(depth // 8, 8, width), axis=0)
+            total = part if low == 0 else total + part
+            term = jnp.dot(vals[:, low : low + depth], expo.astype(BF16), preferred_element_type=F32)
+            gain = term if low == 0 else gain + term
+            if low + depth == keys.shape[0]:
+                sum_ref[:, cols] += total
+                acc_ref[yq, :, cols] += gain
+
+    def fast(yq, carry):
         st_ref[yq, 0:1] = jnp.full((1, lanes), NEG_LARGE, F32)
         st_ref[yq, 1:8] = jnp.zeros((7, lanes), F32)
-        acc_ref[yq] = jnp.zeros((vd, lanes), F32)
-
-        def pair(p, masked):
-            keys = k_all[pl.ds(2 * p, 2)].reshape(2 * rows, 2 * qd)
-            vals = jnp.concatenate([v_all[2 * p], v_all[2 * p + 1]], axis=1)
-            for at in range(0, lanes, width):
-                cols = slice(at, at + width)
-                sc = jnp.dot(keys, qz[:, cols], preferred_element_type=F32)
-                if masked:
-                    lane = lax.broadcasted_iota(jnp.int32, (1, width), 1) + at
-                    lane = jnp.where(lane >= rows, lane - rows, lane)
-                    qpos = lane + (z * ny + yq) * rows
-                    sub = lax.broadcasted_iota(jnp.int32, (2 * rows, 1), 0)
-                    kpos = sub + (2 * p * ny + y) * rows
-                    kpos = jnp.where(sub >= rows, kpos + (ny - 1) * rows, kpos)
+
+        @pl.when(jnp.logical_or(z > 0, yq >= y))
+        def _():
+            set_queries(yq)
+            few = min(128, rows)
+            sc = jnp.dot(k_all[0, 0:few], qz_ref[...], preferred_element_type=F32)
+            kpos = y * rows + lax.broadcasted_iota(jnp.int32, (few, 1), 0)
+            bar = jnp.max(jnp.where(kpos <= positions(yq, 0, lanes), sc, NEG_LARGE), axis=0, keepdims=True)
+            st_ref[yq, 0:1] = bar
+            bar_ref[0:1] = bar * factor
+            sum_ref[...] = jnp.zeros_like(sum_ref)
+
+            def run(count, lo, hi):
+                def body(b, carry):
+                    first = lo + b * count
+                    keys = k_all[pl.ds(first, count)].reshape(count * rows, 2 * qd)
+                    vals = jnp.concatenate([v_all[first + i] for i in range(count)], axis=1)
+                    tiles(yq, keys, vals, None)
+                    return carry
+
+                lax.fori_loop(0, (hi - lo) // count, body, 0)
+                return lo + (hi - lo) // count * count
+
+            blocks = z + jnp.where(yq > y, 1, 0)
+            done = run(4, 0, blocks)
+            done = run(2, done, blocks)
+            run(1, done, blocks)
+
+            @pl.when(yq == y)
+            def _():
+                kpos = (z * ny + y) * rows + lax.broadcasted_iota(jnp.int32, (rows, 1), 0)
+                tiles(yq, k_all[z], v_all[z], lambda at: kpos <= positions(yq, at, width))
+
+            st_ref[yq, 1:2] = jnp.sum(sum_ref[...], axis=0, keepdims=True)
+
+        @pl.when(jnp.logical_and(z == 0, yq < y))
+        def _():
+            acc_ref[yq] = jnp.zeros((vd, lanes), F32)
+
+        return carry
+
+    lax.fori_loop(0, ny, fast, 0)
+    largest = jnp.max(st_ref[:, 1:2])
+
+    @pl.when(jnp.logical_not(largest < 2.0**80))
+    def _():
+        def slow(yq, carry):
+            set_queries(yq)
+            st_ref[yq, 0:1] = jnp.full((1, lanes), NEG_LARGE, F32)
+            st_ref[yq, 1:8] = jnp.zeros((7, lanes), F32)
+
+            def block(b, carry):
+                kpos = (b * ny + y) * rows + lax.broadcasted_iota(jnp.int32, (rows, 1), 0)
+
+                def group(g, carry):
+                    at = pl.multiple_of(g * 128, 128)
+                    cols = pl.ds(at, 128)
+                    lane = lax.broadcasted_iota(jnp.int32, (1, 128), 1) + at
+                    qpos = jnp.where(lane >= rows, lane - rows, lane) + (z * ny + yq) * rows
                     allowed = kpos <= qpos
+                    sc = jnp.dot(k_all[b], qz_ref[:, cols], preferred_element_type=F32)
                     sc = jnp.where(allowed, sc, NEG_LARGE)
-                old = st_ref[yq, 0:1, cols]
-                new = jnp.maximum(old, jnp.max(sc, axis=0, keepdims=True))
-                expo = jnp.exp2((sc - new) * factor)
-                if masked:
-                    expo = jnp.where(allowed, expo, 0.0)
-                shrink = jnp.exp2((old - new) * factor)
-                st_ref[yq, 0:1, cols] = new
-                st_ref[yq, 1:2, cols] = st_ref[yq, 1:2, cols] * shrink + jnp.sum(expo, axis=0, keepdims=True)
-                acc_ref[yq, :, cols] = acc_ref[yq, :, cols] * shrink + jnp.dot(
-                    vals, expo.astype(BF16), preferred_element_type=F32
-                )
-
-        def full(p, carry):
-            pair(p, False)
-            return carry
-
-        lax.fori_loop(0, z // 2, full, 0)
-
-        @pl.when(jnp.logical_or(z % 2 == 1, yq >= y))
-        def _():
-            pair(z // 2, True)
-
-        return 0
-
-    lax.fori_loop(0, ny, chunk, 0)
-
-
-def merge_kernel(ny, scale, acc_ref, st_ref, lam_ref, gain_ref, att_ref, mix, wbuf, sbuf, wland, sland, ws, wr, ss, sr):
+                    old = st_ref[yq, 0:1, cols]
+                    new = jnp.maximum(old, jnp.max(sc, axis=0, keepdims=True))
+                    expo = jnp.where(allowed, jnp.exp2((sc - new) * factor), 0.0)
+                    shrink = jnp.exp2((old - new) * factor)
+                    st_ref[yq, 0:1, cols] = new
+                    st_ref[yq, 1:2, cols] = st_ref[yq, 1:2, cols] * shrink + jnp.sum(expo, axis=0, keepdims=True)
+                    acc_ref[yq, :, cols] = acc_ref[yq, :, cols] * shrink + jnp.dot(
+                        v_all[b], expo.astype(BF16), preferred_element_type=F32
+                    )
+                    return carry
+
+                return lax.fori_loop(0, lanes // 128, group, carry)
+
+            return lax.fori_loop(0, z + 1, block, carry)
+
+        lax.fori_loop(0, ny, slow, 0)
+
+
+def finish_kernel(
+    ny, nx, scale, acc_ref, st_ref, lam_ref, gain_ref, p_ref, halo, gw_ref, ps_ref, wo_ref, out_ref,
+    mix, branch, mine, wbuf, sbuf, wland, sland, give, take, send, land, ws, wr, ss, sr, gs, gr, os, or_,
+):
     s, t = lax.axis_index("sp"), lax.axis_index("tp")
-    z, y = s // ny, s % ny
-    rows = att_ref.shape[0]
+    z, y, x, c = s // ny, s % ny, t // 2, t % 2
+    rows, head = p_ref.shape
+    orows = out_ref.shape[0]
+    chunks, _, width = mine.shape
     factor = scale / math.log(2.0)
     dev = lambda i: (z * ny + i % ny, t)
-    greet([dev(y + 1), dev(y + ny - 1)])
+    partner = (s, x * 2 + 1 - c)
+    across = [(s, ((x + d) % nx) * 2 + c) for d in range(1, nx)]
+    greet([dev(y + 1), dev(y + ny - 1), partner] + across)
+
+    def pooled():
+        here = p_ref[...].astype(F32)
+        rim = jnp.where(s > 0, halo[...].astype(F32), 0.0)
+        total = jnp.concatenate([rim, here], axis=0)
+        slot = t % 4
+        for i in range(4):
+            more = total + pltpu.roll(total, 1 << i, 0)
+            total = jnp.where(i <= slot, more, total)
+        span = jnp.where(slot == 0, 2, jnp.where(slot == 1, 4, jnp.where(slot == 2, 8, 16)))
+        pos = s * rows + lax.broadcasted_iota(jnp.int32, (rows, 1), 0)
+        count = jnp.minimum(pos + 1, span).astype(F32)
+        differ = (total[RIM:] / count - here).astype(BF16)
+        return (jnp.dot(differ, gw_ref[0], preferred_element_type=F32) * ps_ref[...]).astype(BF16)
 
     def own(block, m):
         cols = slice(m * rows, (m + 1) * rows)
@@ -318,6 +434,8 @@
                 sbuf[d, m, k, 1:2] = state[2]
                 for copy in copies(d, m, k):
                     copy.start()
+        if k == 0:
+            branch[:, head:] = pooled()
     for m in range(2):
         state = own(y, m)
         for d in range(2):
@@ -330,60 +448,54 @@
             mix[...] = state[0] / state[2]
         else:
             mix[...] = mix[...] - lam_ref[0:1, 0:1] * state[0] / state[2]
-    head = mix[...]
-    mean = jnp.mean(head * head, axis=0, keepdims=True)
-    normed = jnp.transpose(head * lax.rsqrt(mean + EPSILON)) * gain_ref[...]
-    att_ref[...] = normed.astype(BF16)
+    mixed = mix[...]
+    mean = jnp.mean(mixed * mixed, axis=0, keepdims=True)
+    normed = jnp.transpose(mixed * lax.rsqrt(mean + EPSILON)) * gain_ref[...]
+    branch[:, 0:head] = normed.astype(BF16)
+
+    def rows_of(core):
+        starts = [pl.multiple_of((2 * i + core) * orows, 16) for i in range(nx)]
+        return jnp.concatenate([branch[pl.ds(at, orows)] for at in starts], axis=0)
+
+    def product(lhs, n):
+        return lax.dot_general(
+            lhs, wo_ref[n * width : (n + 1) * width], (((1,), (1,)), ((), ())), preferred_element_type=F32
+        )
+
+    lhs = rows_of(1 - c)
+    gives = [rcopy(give.at[n], take.at[n], gs.at[n], gr.at[n], partner) for n in range(chunks)]
+    for n in range(chunks):
+        give[n] = product(lhs, n).astype(BF16)
+        gives[n].start()
+    lhs = rows_of(c)
+    for n in range(chunks):
+        mine[n] = product(lhs, n)
+    outs = []
+    for n in range(chunks):
+        gives[n].wait_recv()
+        both = mine[n] + take[n].astype(F32)
+        mine[n] = both
+        send[n] = both.astype(BF16)
+        for d in range(1, nx):
+            at = pl.multiple_of(((x + d) % nx) * orows, 16)
+            outs.append(
+                rcopy(send.at[n, pl.ds(at, orows)], land.at[d - 1, n], os.at[d - 1, n], or_.at[d - 1, n], across[d - 1])
+            )
+            outs[-1].start()
+    for n in range(chunks):
+        total = mine[n, pl.ds(pl.multiple_of(x * orows, 16), orows)]
+        for d in range(1, nx):
+            outs[n * (nx - 1) + d - 1].wait_recv()
+            total = total + land[d - 1, n].astype(F32)
+        out_ref[:, n * width : (n + 1) * width] = total.astype(BF16)
+    for copy in gives + outs:
+        copy.wait_send()
     for k in range(ny // 2):
         for m in range(2):
             for d in range(2):
                 if k < hops(ny, d, m):
                     for copy in copies(d, m, k):
                         copy.wait_send()
-
-
-def output_kernel(p_ref, halo, gw_ref, ps_ref, att_ref, wo_ref, out_ref):
-    s, t = lax.axis_index("sp"), lax.axis_index("tp")
-    rows, dim = p_ref.shape
-    here = p_ref[...].astype(F32)
-    rim = jnp.where(s > 0, halo[...].astype(F32), 0.0)
-    ext = jnp.concatenate([rim, here], axis=0)
-    total = ext
-    slot = t % 4
-    for i in range(4):
-        more = total + pltpu.roll(total, 1 << i, 0)
-        total = jnp.where(i <= slot, more, total)
-    span = jnp.where(slot == 0, 2, jnp.where(slot == 1, 4, jnp.where(slot == 2, 8, 16)))
-    pos = s * rows + lax.broadcasted_iota(jnp.int32, (rows, 1), 0)
-    count = jnp.minimum(pos + 1, span).astype(F32)
-    differ = (total[RIM:] / count - here).astype(BF16)
-    pooled = jnp.dot(differ, gw_ref[0], preferred_element_type=F32) * ps_ref[...]
-    branch = jnp.concatenate([att_ref[...], pooled.astype(BF16)], axis=1)
-    cols = wo_ref.shape[0]
-    step = min(cols, 512)
-    for at in range(0, cols, step):
-        out_ref[:, at : at + step] = lax.dot_general(
-            branch, wo_ref[at : at + step], (((1,), (1,)), ((), ())), preferred_element_type=F32
-        ).astype(BF16)
-
-
-def scatter_kernel(tp, part_ref, out_ref, land, ss, rs):
-    s, t = lax.axis_index("sp"), lax.axis_index("tp")
-    rows = out_ref.shape[0]
-    peers = [(s, (t + d) % tp) for d in range(1, tp)]
-    greet(peers)
-    copies = []
-    for d in range(1, tp):
-        start = pl.multiple_of(((t + d) % tp) * rows, 16)
-        copies.append(rcopy(part_ref.at[pl.ds(start, rows)], land.at[d - 1], ss.at[d - 1], rs.at[d - 1], peers[d - 1]))
-        copies[-1].start()
-    total = part_ref[pl.ds(pl.multiple_of(t * rows, 16), rows)].astype(F32)
-    for d in range(1, tp):
-        copies[d - 1].wait_recv()
-        total = total + land[d - 1].astype(F32)
-    out_ref[...] = total.astype(BF16)
-    for copy in copies:
-        copy.wait_send()
 
 
 def local(sp, tp, tokens, pre_gain, w_query, w_key, w_value, w_pool, lambdas, sub_gain, group_weight, pool_scale, w_out):
@@ -397,31 +509,29 @@
     cols = w_out.shape[1]
     scale = 1.0 / math.sqrt(qd // 2)
     dma = pltpu.SemaphoreType.DMA
-    tok = jnp.concatenate([tokens, jnp.broadcast_to(pre_gain[None], (16, part))], axis=0)
-    wcat = jnp.concatenate([w_query, w_key, w_value, w_pool, w_out.T], axis=1)
     tok_full, w_full = call(
         functools.partial(gather_kernel, nz, ny, nx),
-        (tok, wcat),
-        (sds(tp, rows + 16, part), sds(nz, ny, 2, wrows // 2, wcat.shape[1])),
-        [dma((2 * nx,)), dma((2 * nx,)), dma((ny,)), dma((ny,)), dma((nz,)), dma((nz,))]
+        (tokens, pre_gain.reshape(1, part), w_query, w_key, w_value, w_pool),
+        (sds(tp, rows + 16, part), sds(nz, ny, 2, wrows // 2, wide)),
+        [VMEM((rows + 16, part), BF16), VMEM((wrows, wide), BF16)]
+        + [dma((2 * nx,)), dma((2 * nx,)), dma((ny,)), dma((ny,)), dma((nz,)), dma((nz,))]
         + ring_sems(nz, 2)
         + ring_sems(ny, 2),
         cid=0,
         name="gather",
     )
-    w_all = w_full.reshape(sp * wrows, wcat.shape[1])
     qt, k, vt, pool = call(
         functools.partial(project_kernel, tp),
-        (tok_full, w_all),
+        (tok_full, w_full.reshape(sp * wrows, wide)),
         (sds(qd, rows), sds(rows, qd), sds(head, rows), sds(rows, head)),
-        [pltpu.VMEM((rows, tp * part), BF16), pltpu.VMEM((rows, 128), F32)],
+        [VMEM((rows, tp * part), BF16), VMEM((rows, 128), F32)],
         name="project",
     )
-    q_all, k_all, v_all, halo = call(
+    q_all, k_all, v_all, halo, wo_all = call(
         functools.partial(spread_kernel, nz, ny),
-        (qt, k, vt, pool),
-        (sds(ny, qd, rows), sds(nz, rows, qd), sds(nz, head, rows), sds(RIM, head)),
-        ring_sems(nz, 2) + ring_sems(ny, 2) + [dma, dma],
+        (qt, k, vt, pool, w_out.T),
+        (sds(ny, qd, rows), sds(nz, rows, qd), sds(nz, head, rows), sds(RIM, head), sds(nz, ny, cols, qd + head)),
+        ring_sems(nz, 2) + ring_sems(ny, 2) + ring_sems(ny, 2) + [dma((nz,)), dma((nz,)), dma, dma],
         cid=1,
         name="spread",
     )
@@ -429,38 +539,44 @@
         functools.partial(attend_kernel, nz, ny, scale),
         (q_all, k_all, v_all),
         (sds(ny, head, 2 * rows, dtype=F32), sds(ny, 8, 2 * rows, dtype=F32)),
+        [VMEM((qd, 2 * rows), BF16), VMEM((8, 2 * rows), F32), VMEM((8, 2 * rows), F32)],
         name="attend",
     )
     half = ny // 2
-    (att,) = call(
-        functools.partial(merge_kernel, ny, scale),
-        (acc, st, jnp.broadcast_to(lambdas.reshape(1, 1), (8, 128)), sub_gain.reshape(1, head)),
-        (sds(rows, head),),
+    orows = rows // tp
+    chunks, width = 4, sp * cols // 4
+    (out,) = call(
+        functools.partial(finish_kernel, ny, nx, scale),
+        (
+            acc,
+            st,
+            jnp.broadcast_to(lambdas.reshape(1, 1), (8, 128)),
+            sub_gain.reshape(1, head),
+            pool,
+            halo,
+            group_weight,
+            pool_scale.reshape(1, head),
+            wo_all.reshape(sp * cols, qd + head),
+        ),
+        (sds(orows, sp * cols),),
         [
-            pltpu.VMEM((head, rows), F32),
-            pltpu.VMEM((2, 2, half, head, rows), BF16),
-            pltpu.VMEM((2, 2, half, 8, rows), F32),
-            pltpu.VMEM((2, 2, half, head, rows), BF16),
-            pltpu.VMEM((2, 2, half, 8, rows), F32),
+            VMEM((head, rows), F32),
+            VMEM((rows, 2 * head), BF16),
+            VMEM((chunks, nx * orows, width), F32),
+            VMEM((2, 2, half, head, rows), BF16),
+            VMEM((2, 2, half, 8, rows), F32),
+            VMEM((2, 2, half, head, rows), BF16),
+            VMEM((2, 2, half, 8, rows), F32),
+            VMEM((chunks, nx * orows, width), BF16),
+            VMEM((chunks, nx * orows, width), BF16),
+            VMEM((chunks, nx * orows, width), BF16),
+            VMEM((max(nx - 1, 1), chunks, orows, width), BF16),
         ]
-        + [dma((2, 2, half))] * 4,
+        + [dma((2, 2, half))] * 4
+        + [dma((chunks,))] * 2
+        + [dma((nx, chunks))] * 2,
         cid=2,
-        name="merge",
-    )
-    (partial,) = call(
-        output_kernel,
-        (pool, halo, group_weight, pool_scale.reshape(1, head), att, w_all[:, wide:]),
-        (sds(rows, sp * cols),),
-        name="output",
-    )
-    out_rows = rows // tp
-    (out,) = call(
-        functools.partial(scatter_kernel, tp),
-        (partial,),
-        (sds(out_rows, sp * cols),),
-        [pltpu.VMEM((tp - 1, out_rows, sp * cols), BF16), dma((tp - 1,)), dma((tp - 1,))],
-        cid=3,
-        name="scatter",
+        name="finish",
     )
     return out
 

time: 169 us -> 286 us (1.69)
  Pallas kernels: 162 us -> 277 us
    pallas_call x7 -> x5, Pallas kernels: 162 us -> 277 us  [call(): pl.pallas_call(kernel, out_shape=tuple(outs), in_specs=vspec(len(ins)), o...]
where the time goes in v2:
time: 286 us; the launch traced here: 283 us
  Pallas kernels  277 us (97%)
  local copies, waits for them, and re-layouts  5.07 us (2%)
    pallas_call x5, Pallas kernels, call(): pl.pallas_call(kernel, out_shape=tuple(outs), in_specs=vspec(len(ins)), o...  277 us

profile of v2, /device:TPU:449, one launch (start us, length us, event | category | flops | bytes accessed | tf_op | source)
XLA Modules:
  0.0 283.2 jit_solution(15454426082096244858)
XLA Ops:
  0.0 0.7 reshape.17.gain_ref
  0.7 0.0 copy-start
  0.7 0.9 copy-done
  1.6 0.0 copy-start.3
  1.6 0.7 copy-done.3
  2.3 0.0 copy-start.4
  2.3 0.7 copy-done.4
  3.0 0.0 copy-start.5
  3.0 0.7 copy-done.5
  3.7 0.0 copy-start.6
  3.7 0.7 copy-done.6
  4.4 0.0 copy-start.2
  4.4 27.8 %gather.1 = (bf16[8,400,256]{2,1,0:T(8,128)(2,1)S(1)}, bf16[8,8,2,16,512]{4,3,2,1,0:T(8,128)(2,1)S(1)}) custom-call(bf16[384,256]{1,0:T(8,128)(2,1)S(1)} %copy-done, bf16[1,256]{1,0:T(2,128)(2,1)S(1)} %reshape.17.gain_ref, bf16[32,128]{1,0:T(8,128)(2,1)S(1)} %copy-done.3, bf16[32,128]{1,0:T(8,128)(2,1)S(1)} %copy-done.4, bf16[32,128]{1,0:T(8,128)(2,1)S(1)} %copy-done.5, ...), custom_call_target="tpu_custom_call" | custom-call | flops 16777216 | bytes 1048576 | tf_op jit(solution)/shard_map/gather/pallas_call | solution.py:38
  32.2 1.1 project.1
  33.3 0.0 copy-start.1
  33.3 0.0 copy-start.7
  33.4 0.0 copy-start.8
  33.4 0.0 copy-done.2
  33.4 27.3 %spread.1 = (bf16[8,128,384]{2,1,0:T(8,128)(2,1)S(1)}, bf16[8,384,128]{2,1,0:T(8,128)(2,1)S(1)}, bf16[8,128,384]{2,1,0:T(8,128)(2,1)S(1)}, bf16[16,128]{1,0:T(8,128)(2,1)S(1)}, bf16[8,8,32,256]{3,2,1,0:T(8,128)(2,1)S(1)}) custom-call(bf16[128,384]{1,0:T(8,128)(2,1)S(1)} %get-tuple-element.20.q_ref, bf16[384,128]{1,0:T(8,128)(2,1)S(1)} %get-tuple-element.21.k_ref, ...), custom_call_target="tpu_custom_call" | custom-call | flops 16777216 | bytes 1048576 | tf_op jit(solution)/shard_map/spread/pallas_call | solution.py:38
  60.7 23.7 %attend.1 = (f32[8,128,768]{2,1,0:T(8,128)S(1)}, f32[8,8,768]{2,1,0:T(8,128)S(1)}) custom-call(bf16[8,128,384]{2,1,0:T(8,128)(2,1)S(1)} %get-tuple-element.24.q_all, bf16[8,384,128]{2,1,0:T(8,128)(2,1)S(1)} %get-tuple-element.25.k_all, bf16[8,128,384]{2,1,0:T(8,128)(2,1)S(1)} %get-tuple-element.26.v_all), custom_call_target="tpu_custom_call" | custom-call | flops 16777216 | bytes 1048576 | tf_op jit(solution)/shard_map/attend/pallas_call | solution.py:38
  85.0 0.0 copy-done.1
  85.0 0.0 copy-done.7
  85.0 0.0 copy-done.8
  85.1 197.4 %finish.1 = bf16[48,2048]{1,0:T(8,128)(2,1)S(1)} custom-call(f32[8,128,768]{2,1,0:T(8,128)S(1)} %get-tuple-element.27.acc_ref, f32[8,8,768]{2,1,0:T(8,128)S(1)} %get-tuple-element.28.st_ref, f32[8,128]{1,0:T(8,128)S(1)} %broadcast_in_dim.8.lam_ref, f32[1,128]{1,0:T(1,128)S(1)} %bitcast.10, bf16[384,128]{1,0:T(8,128)(2,1)S(1)} %get-tuple-element.23.p_ref, ...), custom_call_target="tpu_custom_call" | custom-call | flops 16777216 | bytes 1048576 | tf_op jit(solution)/shard_map/finish/pallas_call | solution.py:38
  282.5 0.7 copy.14
  (1 shorter events, 0.0 us)
Async XLA Ops:
  0.7 0.9 copy-start
  1.6 0.7 copy-start.3
  2.3 0.7 copy-start.4
  3.0 0.7 copy-start.5
  3.7 0.7 copy-start.6
  4.4 29.0 %copy-start.2 = (bf16[256,32]{0,1:T(8,128)(2,1)S(1)}, bf16[256,32]{0,1:T(8,128)(2,1)}, u32[]{:S(2)}) copy-start(bf16[256,32]{0,1:T(8,128)(2,1)} %param.21) | copy-start | bytes 49156
  33.3 51.7 %copy-start.1 = (bf16[1,128,128]{2,1,0:T(8,128)(2,1)S(1)}, bf16[1,128,128]{2,1,0:T(8,128)(2,1)}, u32[]{:S(2)}) copy-start(bf16[1,128,128]{2,1,0:T(8,128)(2,1)} %gw_ref.1) | copy-start | bytes 98308
  33.3 51.7 %copy-start.7 = (f32[128]{0:T(128)S(1)}, f32[128]{0:T(128)}, u32[]{:S(2)}) copy-start(f32[128]{0:T(128)} %param.18) | copy-start | bytes 1540
  33.4 51.7 %copy-start.8 = (f32[128]{0:T(128)S(1)}, f32[128]{0:T(128)}, u32[]{:S(2)}) copy-start(f32[128]{0:T(128)} %param.20) | copy-start | bytes 1540
